TPU v7x, 32 devices: a whole 2x2x4 slice. The times are simulated.
32 devices in a mesh: sp: 4 (over z), fs: 4 (over y, x), tp: 2 (over core).
Axes of the slice: x: 2, y: 2, z: 4, core: 2. Of those that a mesh axis runs over, the one named last changes fastest.
Arguments:
- tokens: bfloat16 [4, 640, 2048], P('fs', 'sp', 'tp'), may hold values from -6 to 6
- mix_gain: float32 [2048], replicated, may hold values from 0.1 to 1.9
- conv_b_weight: bfloat16 [2048, 1024], P(('sp', 'fs'), 'tp'), may hold values from -0.125 to 0.125
- conv_c_weight: bfloat16 [2048, 1024], P(('sp', 'fs'), 'tp'), may hold values from -0.125 to 0.125
- conv_v_weight: bfloat16 [2048, 1024], P(('sp', 'fs'), 'tp'), may hold values from -0.125 to 0.125
- conv_taps: float32 [3, 1024], P(None, 'tp'), may hold values from -3.5 to 3.5
- query_weight: bfloat16 [2048, 2048], P(('sp', 'fs'), 'tp'), may hold values from -0.125 to 0.125
- query_rope_weight: bfloat16 [2048, 1024], P(('sp', 'fs'), 'tp'), may hold values from -4.5 to 4.5
- latent_weight: bfloat16 [2048, 512], P(('sp', 'fs')), may hold values from -0.125 to 0.125
- key_rope_weight: bfloat16 [2048, 64], replicated, may hold values from -1 to 1
- latent_gain: float32 [512], replicated, may hold values from 0.1 to 1.9
- key_up_weight: bfloat16 [512, 2048], P(None, 'tp'), may hold values from -0.25 to 0.25
- value_up_weight: bfloat16 [512, 2048], P(None, 'tp'), may hold values from -0.25 to 0.25
- head_gain: float32 [2048], P('tp'), may hold values from 0.1 to 1.9
- conv_out_weight: bfloat16 [1024, 2048], P('tp', ('sp', 'fs')), may hold values from -0.109375 to 0.109375
- attn_out_weight: bfloat16 [2048, 2048], P('tp', ('sp', 'fs')), may hold values from -0.109375 to 0.109375
Outputs:
- mixed: bfloat16 [4, 640, 2048], P('fs', ('sp', 'tp'))
All inputs are finite; a program needn't handle non-finite values.
Results may differ from a plain program's by a relative error of at most 0.025.
Values may be sent and summed in bfloat16 or wider, within the bound.
A program may use at most 128 MiB of HBM per device.

v0:
```python
import functools
import math

import jax
import jax.numpy as jnp
from jax import lax
from jax.experimental import pallas as pl
from jax.experimental.pallas import tpu as pltpu
from jax.sharding import PartitionSpec as P

NOPE = 128
ROPE = 64
VD = 128
KVL = 512
SEG = 64


norm_epsilon = 1e-06
rope_theta = 10000.0


def passed_along(block, axis, distance):
    devices = range(lax.axis_size(axis))
    route = [(i - distance, i) for i in devices if i - distance in devices]
    return lax.ppermute(block, axis, route)


def rms_scale(values, gain):
    return (
        values * lax.rsqrt(jnp.mean(values * values, axis=-1, keepdims=True) + norm_epsilon) * gain
    )


def rope_tables(positions):
    half_width = ROPE // 2
    frequency = rope_theta ** (-jnp.arange(half_width, dtype=jnp.float32) * 2.0 / ROPE)
    angles = positions[:, None] * frequency[None, :]
    return (jnp.cos(angles), jnp.sin(angles))


def rotate(values, cosine, sine):
    half_width = ROPE // 2
    first = values[..., :half_width]
    second = values[..., half_width:]
    return jnp.concatenate(
        [first * cosine - second * sine, second * cosine + first * sine], axis=-1
    )


def general_shards(
    tokens,
    mix_gain,
    conv_b_weight,
    conv_c_weight,
    conv_v_weight,
    conv_taps,
    query_weight,
    query_rope_weight,
    latent_weight,
    key_rope_weight,
    latent_gain,
    key_up_weight,
    value_up_weight,
    head_gain,
    conv_out_weight,
    attn_out_weight,
):
    full_rows = lax.all_gather(tokens[0], "tp", axis=1, tiled=True)
    tok_rows = full_rows.shape[0]
    normed = rms_scale(full_rows.astype(jnp.float32), mix_gain).astype(jnp.bfloat16)
    offset = lax.axis_index("sp") * tok_rows
    token_index = offset + jnp.arange(tok_rows, dtype=jnp.int32)
    cosine, sine = rope_tables(token_index.astype(jnp.float32))
    local_heads = query_weight.shape[1] // NOPE
    count_sp = lax.axis_size("sp")
    count_fs = lax.axis_size("fs")
    count_tp = lax.axis_size("tp")
    fs_index = lax.axis_index("fs")
    row_piece = normed.shape[1] // (count_sp * count_fs)
    all_normed = lax.all_gather(normed, "fs", axis=0, tiled=True)
    picked = lax.dynamic_index_in_dim(
        all_normed.reshape(-1, count_sp, count_fs, row_piece), fs_index, 2, keepdims=False
    ).reshape(-1, count_sp * row_piece)
    gathered = (
        lax.all_gather(conv_b_weight, "sp", axis=0, tiled=True),
        lax.all_gather(conv_c_weight, "sp", axis=0, tiled=True),
        lax.all_gather(conv_v_weight, "sp", axis=0, tiled=True),
        lax.all_gather(query_weight, "sp", axis=0, tiled=True),
        lax.all_gather(query_rope_weight, "sp", axis=0, tiled=True),
        lax.all_gather(latent_weight, "sp", axis=0, tiled=True),
    )

    def project_in():
        return jnp.concatenate(
            [jnp.dot(picked, member, preferred_element_type=jnp.float32) for member in gathered],
            axis=1,
        )

    joined = lax.psum_scatter(
        project_in().astype(jnp.bfloat16), "fs", scatter_dimension=0, tiled=True
    ).astype(jnp.float32)
    bounds = []
    running_total = 0
    for member in gathered[:-1]:
        running_total = running_total + member.shape[1]
        bounds.append(running_total)
    sums = tuple(jnp.split(joined, bounds, axis=1))
    latent_raw = sums[5].astype(jnp.bfloat16)
    gate_b = sums[0].astype(jnp.bfloat16)
    gate_c = sums[1].astype(jnp.bfloat16)
    values_v = sums[2].astype(jnp.bfloat16)
    query_nope = sums[3].astype(jnp.bfloat16).reshape(tok_rows, local_heads, NOPE)
    query_rot = rotate(
        sums[4].reshape(tok_rows, local_heads, ROPE), cosine[:, None, :], sine[:, None, :]
    ).astype(jnp.bfloat16)
    latent = rms_scale(latent_raw.astype(jnp.float32), latent_gain).astype(jnp.bfloat16)
    key_rot = rotate(
        jnp.dot(normed, key_rope_weight, preferred_element_type=jnp.float32), cosine, sine
    ).astype(jnp.bfloat16)
    query_latent = jnp.einsum(
        "thn,khn->thk",
        query_nope,
        key_up_weight.reshape(KVL, local_heads, NOPE),
        preferred_element_type=jnp.float32,
    ).astype(jnp.bfloat16)
    attn_scale = (NOPE + ROPE) ** (-0.5)
    product = (gate_c.astype(jnp.float32) * values_v.astype(jnp.float32)).astype(jnp.bfloat16)
    previous = passed_along(product[tok_rows - 2 :], "sp", 1)
    padded = jnp.concatenate([previous, product], axis=0).astype(jnp.float32)
    convolved = (
        conv_taps[0] * padded[0:tok_rows]
        + conv_taps[1] * padded[1 : tok_rows + 1]
        + conv_taps[2] * padded[2 : tok_rows + 2]
    )
    conv_y = (gate_b.astype(jnp.float32) * convolved).astype(jnp.bfloat16)
    query_segment = token_index // SEG
    last_segment = (offset + tok_rows - 1) // SEG

    def key_block(running, latent_block, rot_block, first_key):
        peak_old, denom_old, accum_old = running
        block_rows = latent_block.shape[0]
        scores = (
            jnp.einsum(
                "thk,jk->thj", query_latent, latent_block, preferred_element_type=jnp.float32
            )
            + jnp.einsum("thr,jr->thj", query_rot, rot_block, preferred_element_type=jnp.float32)
        ) * attn_scale
        key_segment = (first_key + jnp.arange(block_rows, dtype=jnp.int32)) // SEG
        allowed = key_segment[None, None, :] <= query_segment[:, None, None]
        peak_new = jnp.maximum(peak_old, jnp.max(jnp.where(allowed, scores, -1e30), axis=-1))
        weights = jnp.where(allowed, jnp.exp(scores - peak_new[..., None]), 0.0)
        rescale = jnp.exp(peak_old - peak_new)
        denom_new = denom_old * rescale + jnp.sum(weights, axis=-1)
        accum_new = accum_old * rescale[..., None] + jnp.einsum(
            "thj,jk->thk",
            weights.astype(jnp.bfloat16),
            latent_block,
            preferred_element_type=jnp.float32,
        )
        return (peak_new, denom_new, accum_new)

    starting = (
        jnp.full((tok_rows, local_heads), -1e30, jnp.float32),
        jnp.zeros((tok_rows, local_heads), jnp.float32),
        jnp.zeros((tok_rows, local_heads, KVL), jnp.float32),
    )
    latent_piece = lax.all_gather(latent, "sp", axis=0, tiled=True)
    rot_piece = lax.all_gather(key_rot, "sp", axis=0, tiled=True)
    piece_rows = latent_piece.shape[0]
    splits = max(1, piece_rows // 512)
    while piece_rows % splits:
        splits = splits - 1
    block_rows = piece_rows // splits

    def visit(state, block_index):
        block_begin = block_index * block_rows
        latent_block = lax.dynamic_slice_in_dim(latent_piece, block_begin, block_rows, 0)
        rot_block = lax.dynamic_slice_in_dim(rot_piece, block_begin, block_rows, 0)
        updated = lax.cond(
            block_begin // SEG <= last_segment,
            lambda inner: key_block(inner, latent_block, rot_block, block_begin),
            lambda inner: inner,
            state,
        )
        return (updated, None)

    peak, denom, accum = lax.scan(visit, starting, jnp.arange(splits, dtype=jnp.int32))[0]
    attended = (accum / denom[..., None]).astype(jnp.bfloat16)
    head_out = jnp.einsum(
        "thk,khv->thv",
        attended,
        value_up_weight.reshape(KVL, local_heads, VD),
        preferred_element_type=jnp.float32,
    )
    normed_heads = rms_scale(head_out, head_gain.reshape(local_heads, VD))
    attn_y = normed_heads.astype(jnp.bfloat16).reshape(tok_rows, local_heads * VD)
    share_rows = tok_rows // count_tp
    conv_all, attn_all = (
        lax.all_gather(conv_y, "fs", axis=0, tiled=True),
        lax.all_gather(attn_y, "fs", axis=0, tiled=True),
    )
    conv_sorted = (
        conv_all.reshape(count_fs, count_tp, share_rows, -1)
        .transpose(1, 0, 2, 3)
        .reshape(count_fs * tok_rows, -1)
    )
    attn_sorted = (
        attn_all.reshape(count_fs, count_tp, share_rows, -1)
        .transpose(1, 0, 2, 3)
        .reshape(count_fs * tok_rows, -1)
    )
    conv_cols_sp, attn_cols_sp = (
        lax.all_gather(conv_out_weight, "sp", axis=1, tiled=True),
        lax.all_gather(attn_out_weight, "sp", axis=1, tiled=True),
    )
    col_sums = lax.psum_scatter(
        (
            jnp.dot(conv_sorted, conv_cols_sp, preferred_element_type=jnp.float32)
            + jnp.dot(attn_sorted, attn_cols_sp, preferred_element_type=jnp.float32)
        ).astype(jnp.bfloat16),
        "tp",
        scatter_dimension=0,
        tiled=True,
    )
    col_piece = conv_cols_sp.shape[1] // count_sp
    outgoing = col_sums.reshape(count_fs, share_rows, count_sp * col_piece)
    arrived = lax.all_to_all(outgoing, "fs", split_axis=0, concat_axis=2, tiled=True)
    result = (
        arrived.reshape(share_rows, count_fs, count_sp, col_piece)
        .transpose(0, 2, 1, 3)
        .reshape(share_rows, count_fs * count_sp * col_piece)
    )
    return result[None]


MESH = pl.DeviceIdType.MESH


class Place:
    def __init__(self):
        self.z = lax.axis_index("sp")
        self.f = lax.axis_index("fs")
        self.c = lax.axis_index("tp")

    def to(self, z=None, f=None, c=None):
        return {
            "sp": self.z if z is None else z,
            "fs": self.f if f is None else f,
            "tp": self.c if c is None else c,
        }


def flip(index, bit):
    digit = (index // bit) % 2
    return index + bit * (1 - 2 * digit)


def remote(src, dst, send, recv, device):
    return pltpu.make_async_remote_copy(
        src_ref=src, dst_ref=dst, send_sem=send, recv_sem=recv, device_id=device, device_id_type=MESH
    )


def greet(devices):
    barrier = pltpu.get_barrier_semaphore()
    for device in devices:
        pl.semaphore_signal(barrier, inc=1, device_id=device, device_id_type=MESH)
    pl.semaphore_wait(barrier, len(devices))


def layer_kernel(
    n,
    turns,
    tok_in,
    params,
    cb,
    cc,
    cv,
    qw,
    qr,
    lw,
    krw_in,
    key_up_in,
    value_up_in,
    co,
    ao,
    out,
    tok,
    normed,
    win,
    wout,
    lat,
    gain,
    krw,
    taps,
    lat_gain,
    key_up,
    value_up,
    head_gain,
    conv_y,
    q_nope,
    q_rot,
    keys,
    values,
    cosine,
    sine,
    part,
    pair,
    moving,
    fetched,
    wsem,
    lsem,
    tsem,
    psem,
    latsem,
    ssem,
    pairsem,
    zsem,
):
    here = Place()
    z, f, c = here.z, here.f, here.c
    fx, fy = flip(f, 1), flip(f, 2)
    other = 1 - c
    rows = cb.shape[0]
    members = (cb, cc, cv, qw, qr, lw)
    widths = [m.shape[1] // n for m in members]
    starts = [sum(widths[:i]) for i in range(len(widths))]
    total = sum(widths)
    lat_w = widths[-1]
    proj_w = total - lat_w
    tr = tok_in.shape[1]
    length = n * tr
    half = length // 2
    outs = (co, ao)
    heights = [m.shape[0] // n for m in outs]
    tops = [sum(heights[:i]) for i in range(len(heights))]
    out_cols = co.shape[1]

    steps = [(1 + j, s) for j in range(n - 1) for s in (-1, 1)]

    greet(
        [here.to(z=lax.rem(z + j, n)) for j in range(1, n)]
        + [here.to(f=fx), here.to(f=fy), here.to(c=other)]
    )

    def in_block(zs, fs):
        return win.at[pl.ds(pl.multiple_of((zs * 4 + fs) * rows, rows), rows), :]

    def out_block(zs, fs):
        return wout.at[:, pl.ds(pl.multiple_of((zs * 4 + fs) * out_cols, out_cols), out_cols)]

    blocks = (in_block, out_block)

    def pieces(kind, dest):
        found = []
        if kind == 0:
            dst = (z * 4 + f) * rows
            for m, w, s in zip(members, widths, starts):
                src = m.at[:, pl.ds(pl.multiple_of(dest * w, w), w)]
                found.append((src, win.at[pl.ds(pl.multiple_of(dst, rows), rows), pl.ds(s, w)]))
        else:
            dst = (z * 4 + f) * out_cols
            for m, h, s in zip(outs, heights, tops):
                src = m.at[pl.ds(pl.multiple_of(dest * h, h), h), :]
                found.append((src, wout.at[pl.ds(s, h), pl.ds(pl.multiple_of(dst, out_cols), out_cols)]))
        return found

    def send_own(kind):
        for src, dst in pieces(kind, z):
            remote(src, dst, wsem.at[kind, 2, z], wsem.at[kind, 3, z], here.to(f=fx)).start()
            remote(src, dst, wsem.at[kind, 4, z], wsem.at[kind, 5, z], here.to(f=fy)).start()
            pltpu.make_async_copy(src, dst, lsem.at[kind]).start()

    def send_z(kind, distance, sign):
        dest = z + sign * distance

        @pl.when((dest >= 0) & (dest < n))
        def _():
            for src, dst in pieces(kind, dest):
                remote(src, dst, wsem.at[kind, 0, dest], wsem.at[kind, 1, z], here.to(z=dest)).start()

    def plane_copy(kind, zs, role, fs, to):
        block = blocks[kind](zs, fs)
        return remote(block, block, wsem.at[kind, role, zs], wsem.at[kind, role + 1, zs], here.to(f=to))

    def relay_z(kind, distance, sign):
        zs = z + sign * distance

        @pl.when((zs >= 0) & (zs < n))
        def _():
            block = blocks[kind](zs, f)
            remote(block, block, wsem.at[kind, 0, zs], wsem.at[kind, 1, zs], here.to(z=zs)).wait_recv()
            plane_copy(kind, zs, 2, f, fx).start()
            plane_copy(kind, zs, 4, f, fy).start()

    def relay_plane(kind, zs):
        plane_copy(kind, zs, 2, fx, fx).wait_recv()

        @pl.when(zs % 2 == 0)
        def _():
            plane_copy(kind, zs, 6, fx, fy).start()

        plane_copy(kind, zs, 4, fy, fy).wait_recv()

        @pl.when(zs % 2 == 1)
        def _():
            plane_copy(kind, zs, 6, fy, fx).start()

    def tok_block(half_index, zs):
        return tok.at[half_index, pl.ds(pl.multiple_of(zs * tr, tr), tr), :]

    def tok_copy(zs, sign, hop, src=None):
        d = (sign + 1) // 2
        block = tok_block(c, zs)
        return remote(
            block if src is None else src, block, tsem.at[d, 0, hop], tsem.at[d, 1, hop], here.to(z=z + sign)
        )

    def partner_copy(zs, owner, src=None):
        block = tok_block(owner, zs)
        return remote(block if src is None else src, block, psem.at[0, zs], psem.at[1, zs], here.to(c=other))

    own_tok = tok_in.at[0]

    def can(sign):
        return (z + sign >= 0) & (z + sign < n)

    channels = widths[0]
    heads = widths[3] // NOPE
    rot_w = widths[4]
    share = tr // 2

    def columns_of(array, width):
        return array.at[:, pl.ds(pl.multiple_of(z * width, width), width)]

    low_w = n * lat_w
    shift_by = pl.multiple_of(low_w + z * heads * VD, 128)
    small = [
        (params, gain),
        (krw_in, krw.at[0:ROPE, :]),
        (krw_in, krw.at[ROPE : 2 * ROPE, :]),
        (columns_of(params, channels), taps),
        (params.at[:, 0:low_w], lat_gain),
        (columns_of(key_up_in, heads * NOPE), key_up),
        (columns_of(value_up_in, heads * VD), value_up),
        (params.at[:, pl.ds(shift_by, heads * VD)], head_gain),
    ]

    send_own(0)
    for distance, sign in steps[:2]:
        send_z(0, distance, sign)
    partner_copy(z, c, own_tok).start()
    pltpu.make_async_copy(own_tok, tok_block(c, z), lsem.at[2]).start()
    for sign in (-1, 1):
        pl.when(can(sign))(lambda sign=sign: tok_copy(z, sign, 0, own_tok).start())
    for distance, sign in steps[2:]:
        send_z(0, distance, sign)
    for i, (src, dst) in enumerate(small):
        pltpu.make_async_copy(src, dst, ssem.at[i]).start()

    def relay_tok(distance, sign):
        zs = z + sign * distance

        @pl.when((zs >= 0) & (zs < n))
        def _():
            tok_copy(zs, -sign, distance - 1).wait_recv()
            if distance < n - 1:
                pl.when(can(-sign))(lambda: tok_copy(zs, -sign, distance).start())
            partner_copy(zs, c).start()

    def each_zs(fn):
        def body(i, carry):
            fn(lax.rem(z + i, n))
            return carry

        lax.fori_loop(0, n, body, 0)

    def at_distance(distance, fn):
        if distance == 0:
            fn(z)
            return
        for sign in (-1, 1):
            zs = z + sign * distance
            pl.when((zs >= 0) & (zs < n))(lambda zs=zs: fn(zs))

    lane = lax.broadcasted_iota(jnp.int32, (tr, rot_w), 1)
    quarter = lane % (ROPE // 2)
    first_half = (lane % ROPE) < ROPE // 2
    frequency = jnp.exp(quarter.astype(jnp.float32) * (-2.0 / ROPE * math.log(rope_theta)))

    def tables(i, carry):
        at = pl.ds(pl.multiple_of(i * tr, tr), tr)
        position = (i * tr + lax.broadcasted_iota(jnp.int32, (tr, rot_w), 0)).astype(jnp.float32)
        angle = position * frequency
        cosine[at, :] = jnp.cos(angle)
        turned = jnp.sin(angle)
        sine[at, :] = jnp.where(first_half, -turned, turned)
        return carry

    lax.fori_loop(0, n, tables, 0)

    def rotated(x, at):
        swapped = jnp.where(
            first_half, pltpu.roll(x, rot_w - ROPE // 2, 1), pltpu.roll(x, ROPE // 2, 1)
        )
        return (x * cosine[at, :] + swapped * sine[at, :]).astype(jnp.bfloat16)

    for i, (src, dst) in enumerate(small):
        pltpu.make_async_copy(src, dst, ssem.at[i]).wait()
    chunk = tr // 2
    wide = tok.shape[2]

    def norm_block(zs):
        partner_copy(zs, other).wait_recv()

        def norm_chunk(i, carry):
            at = pl.ds(pl.multiple_of(zs * tr + i * chunk, chunk), chunk)
            first = tok[0, at, :].astype(jnp.float32)
            second = tok[1, at, :].astype(jnp.float32)
            mean = (
                jnp.sum(first * first, axis=-1, keepdims=True)
                + jnp.sum(second * second, axis=-1, keepdims=True)
            ) / (2 * wide)
            scale = lax.rsqrt(mean + norm_epsilon)
            normed[at, 0:wide] = (first * scale * gain[0:1, 0:wide]).astype(jnp.bfloat16)
            normed[at, wide : 2 * wide] = (second * scale * gain[0:1, wide : 2 * wide]).astype(jnp.bfloat16)
            return carry

        lax.fori_loop(0, 2, norm_chunk, 0)

    pltpu.make_async_copy(own_tok, tok_block(c, z), lsem.at[2]).wait()
    for distance in range(1, n):
        for sign in (-1, 1):
            relay_z(0, distance, sign)
        for sign in (-1, 1):
            relay_tok(distance, sign)
        at_distance(distance - 1, lambda zs: relay_plane(0, zs))
        at_distance(distance - 1, norm_block)
    send_own(1)
    for distance, sign in steps:
        send_z(1, distance, sign)
    at_distance(n - 1, lambda zs: relay_plane(0, zs))
    at_distance(n - 1, norm_block)

    def relay_done(kind, zs):
        plane_copy(kind, zs, 6, flip(fx, 2), fx).wait_recv()

    pltpu.make_async_copy(in_block(z, f), in_block(z, f), lsem.at[0]).wait()
    each_zs(lambda zs: relay_done(0, zs))

    def lat_block(zs, owner):
        return lat.at[zs, pl.ds(pl.multiple_of(owner * half, half), half), :]

    def lat_copy(dest):
        return remote(lat_block(z, c), lat_block(z, c), latsem.at[0, dest], latsem.at[1, z], here.to(z=dest))

    def lat_arrival(zs):
        return remote(lat_block(zs, c), lat_block(zs, c), latsem.at[0, zs], latsem.at[1, zs], here.to(z=zs))

    def lat_partner(zs, owner):
        return remote(
            lat_block(zs, owner), lat_block(zs, owner), latsem.at[2, zs], latsem.at[3, zs], here.to(c=other)
        )

    mine = pl.ds(pl.multiple_of(c * half, half), half)
    lat[z, mine, :] = jnp.dot(
        normed[mine, :], win[:, proj_w:total], preferred_element_type=jnp.float32
    ).astype(jnp.bfloat16)
    for j in range(1, n):
        lat_copy(lax.rem(z + j, n)).start()
    lat_partner(z, c).start()
    for distance in range(1, n):
        for sign in (-1, 1):
            relay_z(1, distance, sign)
        at_distance(distance - 1, lambda zs: relay_plane(1, zs))

    def project(i, carry):
        at = pl.ds(pl.multiple_of(i * tr, tr), tr)
        block = normed[at, :]
        joined = jnp.dot(block, win[:, 0:proj_w], preferred_element_type=jnp.float32)
        gates = joined[:, 0 : 3 * channels].astype(jnp.bfloat16).astype(jnp.float32)
        gate_b = gates[:, 0:channels]
        product = (
            (gates[:, channels : 2 * channels] * gates[:, 2 * channels : 3 * channels])
            .astype(jnp.bfloat16)
            .astype(jnp.float32)
        )
        row = lax.broadcasted_iota(jnp.int32, (tr, channels), 0)
        older, newer = carry
        once = jnp.where(row == 0, newer, pltpu.roll(product, 1, 0))
        twice = jnp.where(row == 0, older, jnp.where(row == 1, newer, pltpu.roll(product, 2, 0)))
        convolved = taps[2:3, :] * twice + taps[3:4, :] * once + taps[4:5, :] * product
        conv_y[at, :] = (gate_b * convolved).astype(jnp.bfloat16)
        start = 3 * channels
        q_nope[at, :] = joined[:, start : start + heads * NOPE].astype(jnp.bfloat16)
        q_rot[at, :] = rotated(joined[:, start + heads * NOPE :], at)
        key_raw = lax.dot_general(
            block, krw[...], (((1,), (1,)), ((), ())), preferred_element_type=jnp.float32
        )
        key_rot = rotated(key_raw, at)
        for h in range(heads):
            keys[h, at, NOPE:] = key_rot
        return product[tr - 2 : tr - 1, :], product[tr - 1 : tr, :]

    nothing = jnp.zeros((1, channels), jnp.float32)
    lax.fori_loop(0, n, project, (nothing, nothing))
    at_distance(n - 1, lambda zs: relay_plane(1, zs))
    for j in range(1, n):
        zs = lax.rem(z + j, n)
        lat_arrival(zs).wait_recv()
        lat_partner(zs, c).start()
    each_zs(lambda zs: lat_partner(zs, other).wait_recv())

    def expand(i, carry):
        at = pl.ds(pl.multiple_of(i * tr, tr), tr)
        raw = jnp.concatenate([lat[k, at, :] for k in range(n)], axis=1).astype(jnp.float32)
        mean = jnp.mean(raw * raw, axis=-1, keepdims=True)
        low = (raw * lax.rsqrt(mean + norm_epsilon) * lat_gain[1:2, :]).astype(jnp.bfloat16)
        wide_keys = jnp.dot(low, key_up[...], preferred_element_type=jnp.float32).astype(jnp.bfloat16)
        for h in range(heads):
            keys[h, at, 0:NOPE] = wide_keys[:, h * NOPE : (h + 1) * NOPE]
        values[at, :] = jnp.dot(low, value_up[...], preferred_element_type=jnp.float32).astype(jnp.bfloat16)
        return carry

    lax.fori_loop(0, n, expand, 0)
    pltpu.make_async_copy(out_block(z, f), out_block(z, f), lsem.at[1]).wait()
    each_zs(lambda zs: relay_done(1, zs))

    shift = SEG.bit_length() - 1
    row_index = lax.broadcasted_iota(jnp.int32, (tr, length), 0)
    key_segment = jnp.right_shift(lax.broadcasted_iota(jnp.int32, (tr, length), 1), shift)
    own_lanes = lane // ROPE

    def block_output(dest):
        at = pl.ds(pl.multiple_of(dest * tr, tr), tr)
        allowed = key_segment <= jnp.right_shift(row_index + dest * tr, shift)
        outputs = [conv_y[at, :]]
        rot = q_rot[at, :]
        for h in range(heads):
            query = jnp.concatenate(
                [
                    q_nope[at, h * NOPE : (h + 1) * NOPE],
                    jnp.where(own_lanes == h, rot, jnp.zeros_like(rot)),
                ],
                axis=1,
            )
            scores = lax.dot_general(
                query, keys[h], (((1,), (1,)), ((), ())), preferred_element_type=jnp.float32
            ) * (NOPE + ROPE) ** (-0.5)
            scores = jnp.where(allowed, scores, -1e30)
            weights = jnp.exp(scores - jnp.max(scores, axis=-1, keepdims=True))
            denom = jnp.sum(weights, axis=-1, keepdims=True)
            head_out = (
                jnp.dot(
                    weights.astype(jnp.bfloat16),
                    values[:, h * VD : (h + 1) * VD],
                    preferred_element_type=jnp.float32,
                )
                / denom
            )
            mean = jnp.mean(head_out * head_out, axis=-1, keepdims=True)
            gained = head_out * lax.rsqrt(mean + norm_epsilon) * head_gain[1:2, h * VD : (h + 1) * VD]
            outputs.append(gained.astype(jnp.bfloat16))
        mixed = jnp.concatenate(outputs, axis=1)
        part[dest] = jnp.dot(mixed, wout[...], preferred_element_type=jnp.float32).astype(jnp.bfloat16)

    def part_rows(dest, core):
        return part.at[dest, pl.ds(pl.multiple_of(core * share, share), share), :]

    def pair_copy(dest):
        return remote(
            part_rows(dest, other), pair.at[dest], pairsem.at[0, dest], pairsem.at[1, dest], here.to(c=other)
        )

    def line_copy(d, dest):
        return remote(
            moving.at[dest],
            fetched.at[d, dest],
            zsem.at[d, 0, dest],
            zsem.at[d, 1, dest],
            here.to(z=z + 2 * d - 1),
        )

    def turn_of(t):
        dest = jnp.int32(0)
        for zz in range(n):
            for tt in range(n):
                dest = jnp.where((z == zz) & (t == tt), turns[zz][tt], dest)
        return dest

    def summed(dest):
        kept = part[dest, pl.ds(pl.multiple_of(c * share, share), share), :]
        return kept.astype(jnp.float32) + pair[dest].astype(jnp.float32)

    def pass_on(dest):
        d = jnp.where(dest > z, 1, 0)
        before = z - (2 * d - 1)
        has = (before >= 0) & (before < n)
        pair_copy(dest).wait_recv()

        @pl.when(has)
        def _():
            line_copy(d, dest).wait_recv()
            moving[dest] = (summed(dest) + fetched[d, dest].astype(jnp.float32)).astype(jnp.bfloat16)

        @pl.when(jnp.logical_not(has))
        def _():
            moving[dest] = summed(dest).astype(jnp.bfloat16)

        line_copy(d, dest).start()

    def turn(t, carry):
        dest = turn_of(t)
        block_output(dest)
        pair_copy(dest).start()
        pl.when(t >= 1)(lambda: pass_on(turn_of(t - 1)))
        return carry

    lax.fori_loop(0, n, turn, 0)
    pair_copy(z).wait_recv()
    low, high = z > 0, z < n - 1

    @pl.when(low)
    def _():
        line_copy(1, z).wait_recv()

    @pl.when(high)
    def _():
        line_copy(0, z).wait_recv()

    @pl.when(low & high)
    def _():
        out[...] = (
            summed(z) + fetched[1, z].astype(jnp.float32) + fetched[0, z].astype(jnp.float32)
        ).astype(jnp.bfloat16)

    @pl.when(jnp.logical_not(low & high))
    def _():
        d = jnp.where(low, 1, 0)
        out[...] = (summed(z) + fetched[d, z].astype(jnp.float32)).astype(jnp.bfloat16)

    for j in range(1, n):
        zs = lax.rem(z + j, n)
        for kind in (0, 1):
            block = blocks[kind](zs, f)
            remote(block, block, wsem.at[kind, 0, zs], wsem.at[kind, 1, zs], here.to(z=zs)).wait_send()
        lat_copy(zs).wait_send()
        line_copy(jnp.where(zs > z, 1, 0), zs).wait_send()

    def sent(zs):
        for kind in (0, 1):
            plane_copy(kind, zs, 2, f, fx).wait_send()
            plane_copy(kind, zs, 4, f, fy).wait_send()
            plane_copy(kind, zs, 6, fx, fy).wait_send()
        partner_copy(zs, c).wait_send()
        lat_partner(zs, c).wait_send()
        pair_copy(zs).wait_send()

    each_zs(sent)
    for sign in (-1, 1):
        pl.when(can(sign))(lambda sign=sign: tok_copy(z, sign, 0).wait_send())
        for distance in range(1, n - 1):
            zs = z - sign * distance
            pl.when((zs >= 0) & (zs < n) & can(sign))(
                lambda sign=sign, distance=distance: tok_copy(z, sign, distance).wait_send()
            )


def split_shards(
    tokens,
    mix_gain,
    conv_b_weight,
    conv_c_weight,
    conv_v_weight,
    conv_taps,
    query_weight,
    query_rope_weight,
    latent_weight,
    key_rope_weight,
    latent_gain,
    key_up_weight,
    value_up_weight,
    head_gain,
    conv_out_weight,
    attn_out_weight,
):
    n = lax.axis_size("sp")
    tr = tokens.shape[1]
    wide = tokens.shape[2]
    length = n * tr
    features = 2 * wide
    heads = query_weight.shape[1] // NOPE // n
    channels = conv_b_weight.shape[1] // n
    lat_w = latent_weight.shape[1] // n
    proj_w = 3 * channels + heads * (NOPE + ROPE)
    out_rows = (conv_out_weight.shape[0] + attn_out_weight.shape[0]) // n
    columns = attn_out_weight.shape[1] * n * 4
    share = tr // 2
    bf16, f32 = jnp.bfloat16, jnp.float32
    turns = [sorted(range(n), key=lambda dest: (-abs(dest - at), dest)) for at in range(n)]
    dma = pltpu.SemaphoreType.DMA

    def row(values):
        return jnp.pad(values, (0, features - values.shape[0]))[None]

    gains = row(jnp.concatenate([latent_gain, head_gain]))
    spare = 8 - 2 - conv_taps.shape[0]
    params = jnp.concatenate(
        [mix_gain[None], gains, jnp.pad(conv_taps, ((0, spare), (0, features - conv_taps.shape[1])))], axis=0
    )
    result = pl.pallas_call(
        functools.partial(layer_kernel, n, turns),
        out_shape=jax.ShapeDtypeStruct((share, columns), bf16),
        in_specs=[pl.BlockSpec(memory_space=pltpu.HBM)] * 13,
        out_specs=pl.BlockSpec(memory_space=pltpu.VMEM),
        scratch_shapes=[
            pltpu.VMEM((2, length, wide), bf16),
            pltpu.VMEM((length, features), bf16),
            pltpu.VMEM((features, proj_w + lat_w), bf16),
            pltpu.VMEM((out_rows, columns), bf16),
            pltpu.VMEM((n, length, lat_w), bf16),
            pltpu.VMEM((8, features), f32),
            pltpu.VMEM((2 * ROPE, features), bf16),
            pltpu.VMEM((8, channels), f32),
            pltpu.VMEM((8, n * lat_w), f32),
            pltpu.VMEM((n * lat_w, heads * NOPE), bf16),
            pltpu.VMEM((n * lat_w, heads * VD), bf16),
            pltpu.VMEM((8, heads * VD), f32),
            pltpu.VMEM((length, channels), bf16),
            pltpu.VMEM((length, heads * NOPE), bf16),
            pltpu.VMEM((length, heads * ROPE), bf16),
            pltpu.VMEM((heads, length, NOPE + 2 * ROPE), bf16),
            pltpu.VMEM((length, heads * VD), bf16),
            pltpu.VMEM((length, heads * ROPE), f32),
            pltpu.VMEM((length, heads * ROPE), f32),
            pltpu.VMEM((n, tr, columns), bf16),
            pltpu.VMEM((n, share, columns), bf16),
            pltpu.VMEM((n, share, columns), bf16),
            pltpu.VMEM((2, n, share, columns), bf16),
            dma((2, 8, n)),
            dma((3,)),
            dma((2, 2, n)),
            dma((2, n)),
            dma((4, n)),
            dma((8,)),
            dma((2, n)),
            dma((2, 2, n)),
        ],
        compiler_params=pltpu.CompilerParams(
            collective_id=0, has_side_effects=True, vmem_limit_bytes=56 * 1024 * 1024
        ),
        name="whole_layer",
    )(
        tokens,
        params,
        conv_b_weight,
        conv_c_weight,
        conv_v_weight,
        query_weight,
        query_rope_weight,
        latent_weight,
        key_rope_weight.T,
        key_up_weight,
        value_up_weight,
        conv_out_weight,
        attn_out_weight,
    )
    return result[None]


def splits_well(mesh):
    n = mesh.shape["sp"]
    return n > 2 and n <= 4 and mesh.shape["fs"] == 4 and mesh.shape["tp"] == 2


def shards(*arrays):
    n = lax.axis_size("sp")
    conv, query, rope, low_rank = (arrays[i].shape[1] for i in (2, 6, 7, 8))
    heads = query // NOPE
    even = heads == n * 128 // ROPE and all(w % (128 * n) == 0 for w in (conv, query, rope, low_rank))
    if even and arrays[0].shape[1] % 32 == 0 and arrays[15].shape[1] % 128 == 0:
        return split_shards(*arrays)
    return general_shards(*arrays)


def solution(mesh):
    return jax.shard_map(
        shards if splits_well(mesh) else general_shards,
        mesh=mesh,
        in_specs=(
            P("fs", "sp", "tp"),
            P(),
            P(("sp", "fs"), "tp"),
            P(("sp", "fs"), "tp"),
            P(("sp", "fs"), "tp"),
            P(None, "tp"),
            P(("sp", "fs"), "tp"),
            P(("sp", "fs"), "tp"),
            P(("sp", "fs"), None),
            P(),
            P(),
            P(None, "tp"),
            P(None, "tp"),
            P("tp"),
            P("tp", ("sp", "fs")),
            P("tp", ("sp", "fs")),
        ),
        out_specs=P("fs", ("sp", "tp"), None),
        check_vma=False,
    )
```

profile of v0, /device:TPU:0, one launch (start us, length us, event | category | flops | bytes accessed | tf_op | source)
XLA Modules:
  0.0 108.6 jit_solution(17179218458524518764)
XLA Ops:
  0.0 0.0 copy-start.2
  0.0 0.0 copy-start.1
  0.0 0.7 copy-done.2
  0.7 0.0 copy-start
  0.7 0.7 select_maximum_fusion.1
  1.4 0.0 copy-done.1
  1.4 0.0 copy-done
  1.4 0.7 select_maximum_fusion.params
  2.0 104.8 %whole_layer.1 = bf16[80,2048]{1,0:T(8,128)(2,1)} custom-call(bf16[1,160,1024]{2,1,0:T(8,128)(2,1)} %tok_in.1, f32[8,2048]{1,0:T(8,128)} %select_maximum_fusion.params, bf16[128,512]{1,0:T(8,128)(2,1)} %cb.1, bf16[128,512]{1,0:T(8,128)(2,1)} %cc.1, bf16[128,512]{1,0:T(8,128)(2,1)} %cv.1, bf16[128,1024]{1,0:T(8,128)(2,1)} %qw.1, bf16[128,512]{1,0:T(8,128)(2,1)} %qr.1, ...), custom_call_target="tpu_custom_call" | custom-call | tf_op jit(solution)/shard_map/whole_layer/pallas_call | solution.py:811
  106.9 1.7 %copy.18 = bf16[1,80,2048]{2,1,0:T(8,128)(2,1)} copy(bf16[1,80,2048]{2,1,0:T(8,128)(2,1)} %bitcast.4) | data formatting | bytes 655360
Async XLA Ops:
  0.0 0.7 copy-start.2
  0.0 1.4 %copy-start.1 = (f32[2048]{0:T(1024)S(1)}, f32[2048]{0:T(1024)}, u32[]{:S(2)}) copy-start(f32[2048]{0:T(1024)} %param.17) | copy-start | bytes 24580
  0.7 0.7 copy-start
where the time goes:
time: 109 us
  Pallas kernels  105 us (96%)
  local copies, waits for them, and re-layouts  2.4 us (2%)
  other arithmetic  1.36 us (1%)
    pallas_call x1, Pallas kernels, split_shards(): pl.pallas_call(functools.partial(layer_kernel, n, turns), out_shape=jax.S...  105 us
    unnamed x7, local copies, waits for them, and re-layouts  2.4 us

commit v1 on v0

--- a/solution.py
+++ b/solution.py
@@ -268,11 +268,26 @@
     pl.semaphore_wait(barrier, len(devices))
 
 
+def orders(n):
+    arrival, compute, passing = [], [], []
+    for z in range(n):
+        first = z + 1 if z < n - 1 else z - 1
+        far = sorted((d for d in range(n) if d != z), key=lambda d: (-abs(d - z), min(d, n - 1 - d)))
+        arrival.append(sorted(range(n), key=lambda d: (abs(d - z), d)))
+        compute.append([first] + sorted((d for d in far if d != first), key=lambda d: -abs(d - z)) + [z])
+        passing.append(far)
+    return arrival, compute, passing
+
+
 def layer_kernel(
     n,
-    turns,
+    parts,
+    order,
     tok_in,
-    params,
+    mix_gain_in,
+    lat_gain_in,
+    head_gain_in,
+    taps_in,
     cb,
     cc,
     cv,
@@ -289,7 +304,9 @@
     normed,
     win,
     wout,
+    wlat,
     lat,
+    krot,
     gain,
     krw,
     taps,
@@ -297,7 +314,8 @@
     key_up,
     value_up,
     head_gain,
-    conv_y,
+    gate,
+    prod,
     q_nope,
     q_rot,
     keys,
@@ -309,6 +327,7 @@
     moving,
     fetched,
     wsem,
+    fsem,
     lsem,
     tsem,
     psem,
@@ -321,22 +340,38 @@
     z, f, c = here.z, here.f, here.c
     fx, fy = flip(f, 1), flip(f, 2)
     other = 1 - c
+    is_end = (z == 0) | (z == n - 1)
     rows = cb.shape[0]
-    members = (cb, cc, cv, qw, qr, lw)
+    members = (cb, cc, cv, qw, qr)
     widths = [m.shape[1] // n for m in members]
     starts = [sum(widths[:i]) for i in range(len(widths))]
-    total = sum(widths)
-    lat_w = widths[-1]
-    proj_w = total - lat_w
+    lat_half = lw.shape[1] // 2
     tr = tok_in.shape[1]
+    hr = tr // 2
     length = n * tr
-    half = length // 2
     outs = (co, ao)
     heights = [m.shape[0] // n for m in outs]
     tops = [sum(heights[:i]) for i in range(len(heights))]
     out_cols = co.shape[1]
+    head_rows = prod.shape[0] - length
 
     steps = [(1 + j, s) for j in range(n - 1) for s in (-1, 1)]
+
+    def chosen(table, t):
+        found = jnp.int32(0)
+        for zz in range(n):
+            for tt in range(len(table[zz])):
+                found = jnp.where((z == zz) & (t == tt), table[zz][tt], found)
+        return found
+
+    def arrive_at(t):
+        return chosen(order[0], t)
+
+    def turn_of(t):
+        return chosen(order[1], t)
+
+    def pass_of(t):
+        return chosen(order[2], t)
 
     greet(
         [here.to(z=lax.rem(z + j, n)) for j in range(1, n)]
@@ -349,7 +384,10 @@
     def out_block(zs, fs):
         return wout.at[:, pl.ds(pl.multiple_of((zs * 4 + fs) * out_cols, out_cols), out_cols)]
 
-    blocks = (in_block, out_block)
+    def low_block(zs, fs):
+        return wlat.at[pl.ds(pl.multiple_of((zs * 4 + fs) * rows, rows), rows), :]
+
+    blocks = (in_block, out_block, low_block)
 
     def pieces(kind, dest):
         found = []
@@ -358,11 +396,13 @@
             for m, w, s in zip(members, widths, starts):
                 src = m.at[:, pl.ds(pl.multiple_of(dest * w, w), w)]
                 found.append((src, win.at[pl.ds(pl.multiple_of(dst, rows), rows), pl.ds(s, w)]))
-        else:
+        elif kind == 1:
             dst = (z * 4 + f) * out_cols
             for m, h, s in zip(outs, heights, tops):
                 src = m.at[pl.ds(pl.multiple_of(dest * h, h), h), :]
                 found.append((src, wout.at[pl.ds(s, h), pl.ds(pl.multiple_of(dst, out_cols), out_cols)]))
+        else:
+            found.append((lw.at[:, pl.ds(pl.multiple_of(c * lat_half, lat_half), lat_half)], low_block(z, f)))
         return found
 
     def send_own(kind):
@@ -371,10 +411,25 @@
             remote(src, dst, wsem.at[kind, 4, z], wsem.at[kind, 5, z], here.to(f=fy)).start()
             pltpu.make_async_copy(src, dst, lsem.at[kind]).start()
 
+    def can(sign):
+        return (z + sign >= 0) & (z + sign < n)
+
+    def within(zs):
+        return (zs >= 0) & (zs < n)
+
+    def reached(distance, sign):
+        dest = z + sign * distance
+        if distance == 1:
+            return within(dest)
+        return (dest > 0) & (dest < n - 1)
+
+    def serves(sign):
+        return z + sign == (n - 1 if sign > 0 else 0)
+
     def send_z(kind, distance, sign):
         dest = z + sign * distance
 
-        @pl.when((dest >= 0) & (dest < n))
+        @pl.when(reached(distance, sign) if kind == 2 else within(dest))
         def _():
             for src, dst in pieces(kind, dest):
                 remote(src, dst, wsem.at[kind, 0, dest], wsem.at[kind, 1, z], here.to(z=dest)).start()
@@ -383,13 +438,19 @@
         block = blocks[kind](zs, fs)
         return remote(block, block, wsem.at[kind, role, zs], wsem.at[kind, role + 1, zs], here.to(f=to))
 
+    def end_copy(zs, sign):
+        block = low_block(zs, f)
+        return remote(block, block, fsem.at[zs], wsem.at[2, 1, zs], here.to(z=z + sign))
+
     def relay_z(kind, distance, sign):
         zs = z + sign * distance
 
-        @pl.when((zs >= 0) & (zs < n))
+        @pl.when(within(zs))
         def _():
             block = blocks[kind](zs, f)
             remote(block, block, wsem.at[kind, 0, zs], wsem.at[kind, 1, zs], here.to(z=zs)).wait_recv()
+            if kind == 2:
+                pl.when(serves(-sign))(lambda: end_copy(zs, -sign).start())
             plane_copy(kind, zs, 2, f, fx).start()
             plane_copy(kind, zs, 4, f, fy).start()
 
@@ -406,24 +467,29 @@
         def _():
             plane_copy(kind, zs, 6, fy, fx).start()
 
-    def tok_block(half_index, zs):
-        return tok.at[half_index, pl.ds(pl.multiple_of(zs * tr, tr), tr), :]
-
-    def tok_copy(zs, sign, hop, src=None):
+    def relay_done(kind, zs):
+        plane_copy(kind, zs, 6, flip(fx, 2), fx).wait_recv()
+
+    def tok_block(owner, zs, i):
+        return tok.at[owner, pl.ds(pl.multiple_of(zs * tr + i * hr, hr), hr), :]
+
+    own_tok = [tok_in.at[0, i * hr : (i + 1) * hr, :] for i in range(2)]
+
+    def tok_copy(zs, sign, hop, i, src=None):
         d = (sign + 1) // 2
-        block = tok_block(c, zs)
+        block = tok_block(c, zs, i)
         return remote(
-            block if src is None else src, block, tsem.at[d, 0, hop], tsem.at[d, 1, hop], here.to(z=z + sign)
+            block if src is None else src, block, tsem.at[d, 0, hop, i], tsem.at[d, 1, hop, i], here.to(z=z + sign)
         )
 
-    def partner_copy(zs, owner, src=None):
-        block = tok_block(owner, zs)
-        return remote(block if src is None else src, block, psem.at[0, zs], psem.at[1, zs], here.to(c=other))
-
-    own_tok = tok_in.at[0]
-
-    def can(sign):
-        return (z + sign >= 0) & (z + sign < n)
+    def partner_copy(zs, owner, i, src=None):
+        block = tok_block(owner, zs, i)
+        return remote(
+            block if src is None else src, block, psem.at[0, zs, i], psem.at[1, zs, i], here.to(c=other)
+        )
+
+    def own_copy(i):
+        return pltpu.make_async_copy(own_tok[i], tok_block(c, z, i), lsem.at[3 + i])
 
     channels = widths[0]
     heads = widths[3] // NOPE
@@ -433,40 +499,58 @@
     def columns_of(array, width):
         return array.at[:, pl.ds(pl.multiple_of(z * width, width), width)]
 
-    low_w = n * lat_w
-    shift_by = pl.multiple_of(low_w + z * heads * VD, 128)
     small = [
-        (params, gain),
+        (mix_gain_in, gain.at[0:1, :]),
         (krw_in, krw.at[0:ROPE, :]),
         (krw_in, krw.at[ROPE : 2 * ROPE, :]),
-        (columns_of(params, channels), taps),
-        (params.at[:, 0:low_w], lat_gain),
+        (taps_in, taps),
+        (lat_gain_in, lat_gain.at[0:1, :]),
         (columns_of(key_up_in, heads * NOPE), key_up),
         (columns_of(value_up_in, heads * VD), value_up),
-        (params.at[:, pl.ds(shift_by, heads * VD)], head_gain),
+        (columns_of(head_gain_in, heads * VD), head_gain.at[0:1, :]),
     ]
 
-    send_own(0)
-    for distance, sign in steps[:2]:
-        send_z(0, distance, sign)
-    partner_copy(z, c, own_tok).start()
-    pltpu.make_async_copy(own_tok, tok_block(c, z), lsem.at[2]).start()
+    send_own(2)
+    for distance, sign in steps:
+        send_z(2, distance, sign)
+    for i in range(2):
+        partner_copy(z, c, i, own_tok[i]).start()
+        own_copy(i).start()
+    for kind in (0, 1):
+        send_own(kind)
+
+    def send_inward(kind, distance, sign):
+        pl.when(jnp.logical_not(serves(sign)))(lambda: send_z(kind, distance, sign))
+
+    def send_outward(kind, sign):
+        pl.when(serves(sign))(lambda: send_z(kind, 1, sign))
+
+    def send_tok(sign):
+        for i in range(2):
+            pl.when(can(sign))(lambda i=i: tok_copy(z, sign, 0, i, own_tok[i]).start())
+
+    for kind in (0, 1):
+        for distance, sign in steps:
+            send_inward(kind, distance, sign)
     for sign in (-1, 1):
-        pl.when(can(sign))(lambda sign=sign: tok_copy(z, sign, 0, own_tok).start())
-    for distance, sign in steps[2:]:
-        send_z(0, distance, sign)
+        pl.when(jnp.logical_not(serves(sign)))(lambda sign=sign: send_tok(sign))
     for i, (src, dst) in enumerate(small):
         pltpu.make_async_copy(src, dst, ssem.at[i]).start()
 
-    def relay_tok(distance, sign):
+    def relay_tok(distance, sign, i):
         zs = z + sign * distance
 
-        @pl.when((zs >= 0) & (zs < n))
+        @pl.when(within(zs))
         def _():
-            tok_copy(zs, -sign, distance - 1).wait_recv()
+            tok_copy(zs, -sign, distance - 1, i).wait_recv()
             if distance < n - 1:
-                pl.when(can(-sign))(lambda: tok_copy(zs, -sign, distance).start())
-            partner_copy(zs, c).start()
+                pl.when(can(-sign))(lambda: tok_copy(zs, -sign, distance, i).start())
+            partner_copy(zs, c, i).start()
+
+    def relay_toks(distance):
+        for i in range(2):
+            for sign in (-1, 1):
+                relay_tok(distance, sign, i)
 
     def each_zs(fn):
         def body(i, carry):
@@ -476,12 +560,9 @@
         lax.fori_loop(0, n, body, 0)
 
     def at_distance(distance, fn):
-        if distance == 0:
-            fn(z)
-            return
         for sign in (-1, 1):
             zs = z + sign * distance
-            pl.when((zs >= 0) & (zs < n))(lambda zs=zs: fn(zs))
+            pl.when(within(zs))(lambda zs=zs: fn(zs))
 
     lane = lax.broadcasted_iota(jnp.int32, (tr, rot_w), 1)
     quarter = lane % (ROPE // 2)
@@ -498,6 +579,7 @@
         return carry
 
     lax.fori_loop(0, n, tables, 0)
+    prod[0:head_rows, :] = jnp.zeros((head_rows, channels), prod.dtype)
 
     def rotated(x, at):
         swapped = jnp.where(
@@ -507,14 +589,14 @@
 
     for i, (src, dst) in enumerate(small):
         pltpu.make_async_copy(src, dst, ssem.at[i]).wait()
-    chunk = tr // 2
     wide = tok.shape[2]
 
     def norm_block(zs):
-        partner_copy(zs, other).wait_recv()
+        for i in range(2):
+            partner_copy(zs, other, i).wait_recv()
 
         def norm_chunk(i, carry):
-            at = pl.ds(pl.multiple_of(zs * tr + i * chunk, chunk), chunk)
+            at = pl.ds(pl.multiple_of(zs * tr + i * hr, hr), hr)
             first = tok[0, at, :].astype(jnp.float32)
             second = tok[1, at, :].astype(jnp.float32)
             mean = (
@@ -528,113 +610,174 @@
 
         lax.fori_loop(0, 2, norm_chunk, 0)
 
-    pltpu.make_async_copy(own_tok, tok_block(c, z), lsem.at[2]).wait()
+    def rows_of(zs):
+        return pl.ds(pl.multiple_of(zs * tr, tr), tr)
+
+    def lat_block(zs, owner):
+        return lat.at[owner, rows_of(zs), :]
+
+    def rot_block(zs, owner):
+        return krot.at[pl.ds(pl.multiple_of(zs * tr + owner * hr, hr), hr), :]
+
+    shared = (lat_block, rot_block)
+
+    def lat_copy(k, dest):
+        block = shared[k](z, c)
+        return remote(block, block, latsem.at[k, 0, dest], latsem.at[k, 1, z], here.to(z=dest))
+
+    def lat_arrival(k, zs):
+        block = shared[k](zs, c)
+        return remote(block, block, latsem.at[k, 0, zs], latsem.at[k, 1, zs], here.to(z=zs))
+
+    def lat_forward(k, zs, sign):
+        block = shared[k](zs, c)
+        return remote(block, block, latsem.at[k, 4, zs], latsem.at[k, 1, zs], here.to(z=z + sign))
+
+    def lat_partner(k, zs, owner):
+        block = shared[k](zs, owner)
+        return remote(block, block, latsem.at[k, 2, zs], latsem.at[k, 3, zs], here.to(c=other))
+
+    def relay_lat(distance):
+        for sign in (-1, 1):
+            zs = z + sign * distance
+
+            @pl.when(within(zs))
+            def _(zs=zs, sign=sign):
+                for k in range(2):
+                    lat_arrival(k, zs).wait_recv()
+                    pl.when(serves(-sign))(lambda k=k: lat_forward(k, zs, -sign).start())
+                    lat_partner(k, zs, c).start()
+
+    def own_latents():
+        at = rows_of(z)
+        block = normed[at, :]
+        lat[c, at, :] = jnp.dot(block, wlat[...], preferred_element_type=jnp.float32).astype(jnp.bfloat16)
+        key_raw = lax.dot_general(
+            block, krw[...], (((1,), (1,)), ((), ())), preferred_element_type=jnp.float32
+        )
+        krot[at, :] = rotated(key_raw, at)
+
+    def relay_weights_z(distance):
+        for sign in (-1, 1):
+            for kind in (0, 1):
+                relay_z(kind, distance, sign)
+
+    def relay_weights_plane(zs):
+        for kind in (0, 1):
+            relay_plane(kind, zs)
+
+    for sign in (-1, 1):
+        relay_z(2, 1, sign)
+    relay_plane(2, z)
+    pl.when(jnp.logical_not(is_end))(lambda: [relay_z(2, 2, sign) for sign in (-1, 1)] and None)
+    for sign in (-1, 1):
+        for kind in (0, 1):
+            send_outward(kind, sign)
+        pl.when(serves(sign))(lambda sign=sign: send_tok(sign))
+    for i in range(2):
+        own_copy(i).wait()
+    norm_block(z)
+    pl.when(is_end)(lambda: [relay_z(2, 2, sign) for sign in (-1, 1)] and None)
+    for distance in range(3, n):
+        for sign in (-1, 1):
+            relay_z(2, distance, sign)
+    relay_plane(0, z)
+    relay_plane(1, z)
+    for sign in (-1, 1):
+        relay_z(0, 1, sign)
     for distance in range(1, n):
+        at_distance(distance, lambda zs: relay_plane(2, zs))
+    for sign in (-1, 1):
+        relay_z(0, 2, sign)
+    at_distance(1, lambda zs: relay_plane(0, zs))
+    pltpu.make_async_copy(low_block(z, f), low_block(z, f), lsem.at[2]).wait()
+    each_zs(lambda zs: relay_done(2, zs))
+    own_latents()
+    for distance, sign in steps:
+        dest = z + sign * distance
+
+        @pl.when(reached(distance, sign))
+        def _(dest=dest):
+            for k in range(2):
+                lat_copy(k, dest).start()
+
+    lat_partner(0, z, c).start()
+    for distance in range(3, n):
         for sign in (-1, 1):
             relay_z(0, distance, sign)
-        for sign in (-1, 1):
-            relay_tok(distance, sign)
-        at_distance(distance - 1, lambda zs: relay_plane(0, zs))
-        at_distance(distance - 1, norm_block)
-    send_own(1)
-    for distance, sign in steps:
-        send_z(1, distance, sign)
-    at_distance(n - 1, lambda zs: relay_plane(0, zs))
-    at_distance(n - 1, norm_block)
-
-    def relay_done(kind, zs):
-        plane_copy(kind, zs, 6, flip(fx, 2), fx).wait_recv()
-
-    pltpu.make_async_copy(in_block(z, f), in_block(z, f), lsem.at[0]).wait()
-    each_zs(lambda zs: relay_done(0, zs))
-
-    def lat_block(zs, owner):
-        return lat.at[zs, pl.ds(pl.multiple_of(owner * half, half), half), :]
-
-    def lat_copy(dest):
-        return remote(lat_block(z, c), lat_block(z, c), latsem.at[0, dest], latsem.at[1, z], here.to(z=dest))
-
-    def lat_arrival(zs):
-        return remote(lat_block(zs, c), lat_block(zs, c), latsem.at[0, zs], latsem.at[1, zs], here.to(z=zs))
-
-    def lat_partner(zs, owner):
-        return remote(
-            lat_block(zs, owner), lat_block(zs, owner), latsem.at[2, zs], latsem.at[3, zs], here.to(c=other)
-        )
-
-    mine = pl.ds(pl.multiple_of(c * half, half), half)
-    lat[z, mine, :] = jnp.dot(
-        normed[mine, :], win[:, proj_w:total], preferred_element_type=jnp.float32
-    ).astype(jnp.bfloat16)
-    for j in range(1, n):
-        lat_copy(lax.rem(z + j, n)).start()
-    lat_partner(z, c).start()
-    for distance in range(1, n):
+    for sign in (-1, 1):
+        relay_z(1, 1, sign)
+    for sign in (-1, 1):
+        relay_z(1, 2, sign)
+    at_distance(2, lambda zs: relay_plane(0, zs))
+    for distance in range(3, n):
         for sign in (-1, 1):
             relay_z(1, distance, sign)
-        at_distance(distance - 1, lambda zs: relay_plane(1, zs))
-
-    def project(i, carry):
-        at = pl.ds(pl.multiple_of(i * tr, tr), tr)
-        block = normed[at, :]
-        joined = jnp.dot(block, win[:, 0:proj_w], preferred_element_type=jnp.float32)
-        gates = joined[:, 0 : 3 * channels].astype(jnp.bfloat16).astype(jnp.float32)
-        gate_b = gates[:, 0:channels]
-        product = (
-            (gates[:, channels : 2 * channels] * gates[:, 2 * channels : 3 * channels])
-            .astype(jnp.bfloat16)
-            .astype(jnp.float32)
-        )
-        row = lax.broadcasted_iota(jnp.int32, (tr, channels), 0)
-        older, newer = carry
-        once = jnp.where(row == 0, newer, pltpu.roll(product, 1, 0))
-        twice = jnp.where(row == 0, older, jnp.where(row == 1, newer, pltpu.roll(product, 2, 0)))
-        convolved = taps[2:3, :] * twice + taps[3:4, :] * once + taps[4:5, :] * product
-        conv_y[at, :] = (gate_b * convolved).astype(jnp.bfloat16)
+    relay_toks(1)
+    at_distance(1, lambda zs: relay_plane(1, zs))
+    norm_block(arrive_at(1))
+    relay_lat(1)
+    for distance in range(3, n):
+        at_distance(distance, lambda zs: relay_plane(0, zs))
+    at_distance(2, lambda zs: relay_plane(1, zs))
+    relay_lat(2)
+    relay_toks(2)
+    for distance in range(3, n):
+        at_distance(distance, lambda zs: relay_plane(1, zs))
+        relay_lat(distance)
+    for t in range(2, n - 1):
+        norm_block(arrive_at(t))
+
+    def lat_waits(zs):
+        lat_partner(0, zs, other).wait_recv()
+        pl.when(zs != z)(lambda: lat_partner(1, zs, other).wait_recv())
+
+    def expand(i, carry):
+        lat_waits(i)
+        at = rows_of(i)
+        raw = jnp.concatenate([lat[0, at, :], lat[1, at, :]], axis=1).astype(jnp.float32)
+        mean = jnp.mean(raw * raw, axis=-1, keepdims=True)
+        low = (raw * lax.rsqrt(mean + norm_epsilon) * lat_gain[0:1, :]).astype(jnp.bfloat16)
+        wide_keys = jnp.dot(low, key_up[...], preferred_element_type=jnp.float32).astype(jnp.bfloat16)
+        key_rot = krot[at, :]
+        for h in range(heads):
+            keys[h, at, 0:NOPE] = wide_keys[:, h * NOPE : (h + 1) * NOPE]
+            keys[h, at, NOPE:] = key_rot
+        values[at, :] = jnp.dot(low, value_up[...], preferred_element_type=jnp.float32).astype(jnp.bfloat16)
+        return carry
+
+    lax.fori_loop(0, n, expand, 0)
+    for kind in (0, 1):
+        pltpu.make_async_copy(blocks[kind](z, f), blocks[kind](z, f), lsem.at[kind]).wait()
+    each_zs(lambda zs: [relay_done(kind, zs) for kind in (0, 1)] and None)
+
+    def project(zs):
+        at = rows_of(zs)
+        joined = jnp.dot(normed[at, :], win[...], preferred_element_type=jnp.float32)
+        gates = joined[:, channels : 3 * channels].astype(jnp.bfloat16).astype(jnp.float32)
+        gate[at, :] = joined[:, 0:channels].astype(jnp.bfloat16)
+        below = pl.ds(pl.multiple_of(zs * tr + head_rows, head_rows), tr)
+        prod[below, :] = (gates[:, 0:channels] * gates[:, channels : 2 * channels]).astype(jnp.bfloat16)
         start = 3 * channels
         q_nope[at, :] = joined[:, start : start + heads * NOPE].astype(jnp.bfloat16)
         q_rot[at, :] = rotated(joined[:, start + heads * NOPE :], at)
-        key_raw = lax.dot_general(
-            block, krw[...], (((1,), (1,)), ((), ())), preferred_element_type=jnp.float32
-        )
-        key_rot = rotated(key_raw, at)
-        for h in range(heads):
-            keys[h, at, NOPE:] = key_rot
-        return product[tr - 2 : tr - 1, :], product[tr - 1 : tr, :]
-
-    nothing = jnp.zeros((1, channels), jnp.float32)
-    lax.fori_loop(0, n, project, (nothing, nothing))
-    at_distance(n - 1, lambda zs: relay_plane(1, zs))
-    for j in range(1, n):
-        zs = lax.rem(z + j, n)
-        lat_arrival(zs).wait_recv()
-        lat_partner(zs, c).start()
-    each_zs(lambda zs: lat_partner(zs, other).wait_recv())
-
-    def expand(i, carry):
-        at = pl.ds(pl.multiple_of(i * tr, tr), tr)
-        raw = jnp.concatenate([lat[k, at, :] for k in range(n)], axis=1).astype(jnp.float32)
-        mean = jnp.mean(raw * raw, axis=-1, keepdims=True)
-        low = (raw * lax.rsqrt(mean + norm_epsilon) * lat_gain[1:2, :]).astype(jnp.bfloat16)
-        wide_keys = jnp.dot(low, key_up[...], preferred_element_type=jnp.float32).astype(jnp.bfloat16)
-        for h in range(heads):
-            keys[h, at, 0:NOPE] = wide_keys[:, h * NOPE : (h + 1) * NOPE]
-        values[at, :] = jnp.dot(low, value_up[...], preferred_element_type=jnp.float32).astype(jnp.bfloat16)
-        return carry
-
-    lax.fori_loop(0, n, expand, 0)
-    pltpu.make_async_copy(out_block(z, f), out_block(z, f), lsem.at[1]).wait()
-    each_zs(lambda zs: relay_done(1, zs))
 
     shift = SEG.bit_length() - 1
     row_index = lax.broadcasted_iota(jnp.int32, (tr, length), 0)
     key_segment = jnp.right_shift(lax.broadcasted_iota(jnp.int32, (tr, length), 1), shift)
     own_lanes = lane // ROPE
+    own_channels = pl.ds(pl.multiple_of(z * channels, channels), channels)
 
     def block_output(dest):
-        at = pl.ds(pl.multiple_of(dest * tr, tr), tr)
+        at = rows_of(dest)
         allowed = key_segment <= jnp.right_shift(row_index + dest * tr, shift)
-        outputs = [conv_y[at, :]]
+        padded = prod[pl.ds(pl.multiple_of(dest * tr, head_rows), tr + head_rows), :].astype(jnp.float32)
+        convolved = (
+            taps[0:1, own_channels] * pltpu.roll(padded, 2, 0)[head_rows:]
+            + taps[1:2, own_channels] * pltpu.roll(padded, 1, 0)[head_rows:]
+            + taps[2:3, own_channels] * padded[head_rows:]
+        )
+        outputs = [(gate[at, :].astype(jnp.float32) * convolved).astype(jnp.bfloat16)]
         rot = q_rot[at, :]
         for h in range(heads):
             query = jnp.concatenate(
@@ -659,7 +802,7 @@
                 / denom
             )
             mean = jnp.mean(head_out * head_out, axis=-1, keepdims=True)
-            gained = head_out * lax.rsqrt(mean + norm_epsilon) * head_gain[1:2, h * VD : (h + 1) * VD]
+            gained = head_out * lax.rsqrt(mean + norm_epsilon) * head_gain[0:1, h * VD : (h + 1) * VD]
             outputs.append(gained.astype(jnp.bfloat16))
         mixed = jnp.concatenate(outputs, axis=1)
         part[dest] = jnp.dot(mixed, wout[...], preferred_element_type=jnp.float32).astype(jnp.bfloat16)
@@ -672,98 +815,137 @@
             part_rows(dest, other), pair.at[dest], pairsem.at[0, dest], pairsem.at[1, dest], here.to(c=other)
         )
 
-    def line_copy(d, dest):
+    piece_w = out.shape[1] // parts
+
+    def cut(g):
+        return slice(g * piece_w, (g + 1) * piece_w)
+
+    def line_copy(d, dest, g):
         return remote(
-            moving.at[dest],
-            fetched.at[d, dest],
-            zsem.at[d, 0, dest],
-            zsem.at[d, 1, dest],
+            moving.at[dest, :, cut(g)],
+            fetched.at[d, dest, :, cut(g)],
+            zsem.at[d, 0, dest, g],
+            zsem.at[d, 1, dest, g],
             here.to(z=z + 2 * d - 1),
         )
 
-    def turn_of(t):
-        dest = jnp.int32(0)
-        for zz in range(n):
-            for tt in range(n):
-                dest = jnp.where((z == zz) & (t == tt), turns[zz][tt], dest)
-        return dest
-
-    def summed(dest):
-        kept = part[dest, pl.ds(pl.multiple_of(c * share, share), share), :]
-        return kept.astype(jnp.float32) + pair[dest].astype(jnp.float32)
+    def summed(dest, g):
+        kept = part[dest, pl.ds(pl.multiple_of(c * share, share), share), cut(g)]
+        return kept.astype(jnp.float32) + pair[dest, :, cut(g)].astype(jnp.float32)
+
+    def toward(dest):
+        return jnp.where(dest > z, 1, 0)
+
+    def pass_first(dest):
+        pair_copy(dest).wait_recv()
+        for g in range(parts):
+            moving[dest, :, cut(g)] = summed(dest, g).astype(jnp.bfloat16)
+            line_copy(toward(dest), dest, g).start()
 
     def pass_on(dest):
-        d = jnp.where(dest > z, 1, 0)
-        before = z - (2 * d - 1)
-        has = (before >= 0) & (before < n)
+        d = toward(dest)
         pair_copy(dest).wait_recv()
-
-        @pl.when(has)
+        for g in range(parts):
+            line_copy(d, dest, g).wait_recv()
+            moving[dest, :, cut(g)] = (
+                summed(dest, g) + fetched[d, dest, :, cut(g)].astype(jnp.float32)
+            ).astype(jnp.bfloat16)
+            line_copy(d, dest, g).start()
+
+    def project_arrived(t, carry):
+        project(arrive_at(t))
+        return carry
+
+    lax.fori_loop(0, n - 1, project_arrived, 0)
+
+    def turn(t, carry):
+        @pl.when(t == 1)
         def _():
-            line_copy(d, dest).wait_recv()
-            moving[dest] = (summed(dest) + fetched[d, dest].astype(jnp.float32)).astype(jnp.bfloat16)
-
-        @pl.when(jnp.logical_not(has))
-        def _():
-            moving[dest] = summed(dest).astype(jnp.bfloat16)
-
-        line_copy(d, dest).start()
-
-    def turn(t, carry):
+            pl.when(is_end)(lambda: pass_first(turn_of(0)))
+            for distance in range(3, n):
+                relay_toks(distance)
+            last = arrive_at(n - 1)
+            norm_block(last)
+            project(last)
+
         dest = turn_of(t)
         block_output(dest)
         pair_copy(dest).start()
-        pl.when(t >= 1)(lambda: pass_on(turn_of(t - 1)))
+        pl.when((t >= 2) & is_end)(lambda: pass_first(turn_of(t - 1)))
         return carry
 
     lax.fori_loop(0, n, turn, 0)
+
+    @pl.when(jnp.logical_not(is_end))
+    def _():
+        def passing(t, carry):
+            pass_on(pass_of(t))
+            return carry
+
+        lax.fori_loop(0, n - 1, passing, 0)
+
     pair_copy(z).wait_recv()
     low, high = z > 0, z < n - 1
-
-    @pl.when(low)
-    def _():
-        line_copy(1, z).wait_recv()
-
-    @pl.when(high)
-    def _():
-        line_copy(0, z).wait_recv()
-
-    @pl.when(low & high)
-    def _():
-        out[...] = (
-            summed(z) + fetched[1, z].astype(jnp.float32) + fetched[0, z].astype(jnp.float32)
-        ).astype(jnp.bfloat16)
-
-    @pl.when(jnp.logical_not(low & high))
-    def _():
-        d = jnp.where(low, 1, 0)
-        out[...] = (summed(z) + fetched[d, z].astype(jnp.float32)).astype(jnp.bfloat16)
+    for g in range(parts):
+        pl.when(low)(lambda: line_copy(1, z, g).wait_recv())
+        pl.when(high)(lambda: line_copy(0, z, g).wait_recv())
+
+        @pl.when(low & high)
+        def _():
+            out[:, cut(g)] = (
+                summed(z, g)
+                + fetched[1, z, :, cut(g)].astype(jnp.float32)
+                + fetched[0, z, :, cut(g)].astype(jnp.float32)
+            ).astype(jnp.bfloat16)
+
+        @pl.when(jnp.logical_not(low & high))
+        def _():
+            d = jnp.where(low, 1, 0)
+            out[:, cut(g)] = (summed(z, g) + fetched[d, z, :, cut(g)].astype(jnp.float32)).astype(jnp.bfloat16)
 
     for j in range(1, n):
         zs = lax.rem(z + j, n)
         for kind in (0, 1):
             block = blocks[kind](zs, f)
             remote(block, block, wsem.at[kind, 0, zs], wsem.at[kind, 1, zs], here.to(z=zs)).wait_send()
-        lat_copy(zs).wait_send()
-        line_copy(jnp.where(zs > z, 1, 0), zs).wait_send()
+        for g in range(parts):
+            line_copy(toward(zs), zs, g).wait_send()
+        lat_partner(1, zs, c).wait_send()
+    for distance, sign in steps:
+        dest = z + sign * distance
+
+        @pl.when(reached(distance, sign))
+        def _(dest=dest):
+            block = low_block(dest, f)
+            remote(block, block, wsem.at[2, 0, dest], wsem.at[2, 1, dest], here.to(z=dest)).wait_send()
+            for k in range(2):
+                lat_copy(k, dest).wait_send()
+
+        @pl.when(within(dest) & serves(-sign))
+        def _(dest=dest, sign=sign):
+            end_copy(dest, -sign).wait_send()
+            for k in range(2):
+                lat_forward(k, dest, -sign).wait_send()
 
     def sent(zs):
-        for kind in (0, 1):
+        for kind in (0, 1, 2):
             plane_copy(kind, zs, 2, f, fx).wait_send()
             plane_copy(kind, zs, 4, f, fy).wait_send()
             plane_copy(kind, zs, 6, fx, fy).wait_send()
-        partner_copy(zs, c).wait_send()
-        lat_partner(zs, c).wait_send()
+        for i in range(2):
+            partner_copy(zs, c, i).wait_send()
+        lat_partner(0, zs, c).wait_send()
         pair_copy(zs).wait_send()
 
     each_zs(sent)
     for sign in (-1, 1):
-        pl.when(can(sign))(lambda sign=sign: tok_copy(z, sign, 0).wait_send())
-        for distance in range(1, n - 1):
-            zs = z - sign * distance
-            pl.when((zs >= 0) & (zs < n) & can(sign))(
-                lambda sign=sign, distance=distance: tok_copy(z, sign, distance).wait_send()
-            )
+        for i in range(2):
+            pl.when(can(sign))(lambda sign=sign, i=i: tok_copy(z, sign, 0, i).wait_send())
+            for distance in range(1, n - 1):
+                zs = z - sign * distance
+                pl.when(within(zs) & can(sign))(
+                    lambda sign=sign, distance=distance, i=i: tok_copy(z, sign, distance, i).wait_send()
+                )
 
 
 def split_shards(
@@ -791,42 +973,37 @@
     features = 2 * wide
     heads = query_weight.shape[1] // NOPE // n
     channels = conv_b_weight.shape[1] // n
-    lat_w = latent_weight.shape[1] // n
+    low_rank = latent_weight.shape[1]
     proj_w = 3 * channels + heads * (NOPE + ROPE)
     out_rows = (conv_out_weight.shape[0] + attn_out_weight.shape[0]) // n
     columns = attn_out_weight.shape[1] * n * 4
     share = tr // 2
+    parts = 4
+    head_rows = 16
     bf16, f32 = jnp.bfloat16, jnp.float32
-    turns = [sorted(range(n), key=lambda dest: (-abs(dest - at), dest)) for at in range(n)]
     dma = pltpu.SemaphoreType.DMA
-
-    def row(values):
-        return jnp.pad(values, (0, features - values.shape[0]))[None]
-
-    gains = row(jnp.concatenate([latent_gain, head_gain]))
-    spare = 8 - 2 - conv_taps.shape[0]
-    params = jnp.concatenate(
-        [mix_gain[None], gains, jnp.pad(conv_taps, ((0, spare), (0, features - conv_taps.shape[1])))], axis=0
-    )
     result = pl.pallas_call(
-        functools.partial(layer_kernel, n, turns),
+        functools.partial(layer_kernel, n, parts, orders(n)),
         out_shape=jax.ShapeDtypeStruct((share, columns), bf16),
-        in_specs=[pl.BlockSpec(memory_space=pltpu.HBM)] * 13,
+        in_specs=[pl.BlockSpec(memory_space=pltpu.HBM)] * 16,
         out_specs=pl.BlockSpec(memory_space=pltpu.VMEM),
         scratch_shapes=[
             pltpu.VMEM((2, length, wide), bf16),
             pltpu.VMEM((length, features), bf16),
-            pltpu.VMEM((features, proj_w + lat_w), bf16),
+            pltpu.VMEM((features, proj_w), bf16),
             pltpu.VMEM((out_rows, columns), bf16),
-            pltpu.VMEM((n, length, lat_w), bf16),
+            pltpu.VMEM((features, low_rank // 2), bf16),
+            pltpu.VMEM((2, length, low_rank // 2), bf16),
+            pltpu.VMEM((length, 2 * ROPE), bf16),
             pltpu.VMEM((8, features), f32),
             pltpu.VMEM((2 * ROPE, features), bf16),
-            pltpu.VMEM((8, channels), f32),
-            pltpu.VMEM((8, n * lat_w), f32),
-            pltpu.VMEM((n * lat_w, heads * NOPE), bf16),
-            pltpu.VMEM((n * lat_w, heads * VD), bf16),
+            pltpu.VMEM(conv_taps.shape, f32),
+            pltpu.VMEM((8, low_rank), f32),
+            pltpu.VMEM((low_rank, heads * NOPE), bf16),
+            pltpu.VMEM((low_rank, heads * VD), bf16),
             pltpu.VMEM((8, heads * VD), f32),
             pltpu.VMEM((length, channels), bf16),
+            pltpu.VMEM((length + head_rows, channels), bf16),
             pltpu.VMEM((length, heads * NOPE), bf16),
             pltpu.VMEM((length, heads * ROPE), bf16),
             pltpu.VMEM((heads, length, NOPE + 2 * ROPE), bf16),
@@ -837,22 +1014,26 @@
             pltpu.VMEM((n, share, columns), bf16),
             pltpu.VMEM((n, share, columns), bf16),
             pltpu.VMEM((2, n, share, columns), bf16),
-            dma((2, 8, n)),
-            dma((3,)),
-            dma((2, 2, n)),
-            dma((2, n)),
-            dma((4, n)),
+            dma((3, 8, n)),
+            dma((n,)),
+            dma((5,)),
+            dma((2, 2, n, 2)),
+            dma((2, n, 2)),
+            dma((2, 5, n)),
             dma((8,)),
             dma((2, n)),
-            dma((2, 2, n)),
+            dma((2, 2, n, parts)),
         ],
         compiler_params=pltpu.CompilerParams(
-            collective_id=0, has_side_effects=True, vmem_limit_bytes=56 * 1024 * 1024
+            collective_id=0, has_side_effects=True, vmem_limit_bytes=60 * 1024 * 1024
         ),
         name="whole_layer",
     )(
         tokens,
-        params,
+        mix_gain[None],
+        latent_gain[None],
+        head_gain[None],
+        conv_taps,
         conv_b_weight,
         conv_c_weight,
         conv_v_weight,
@@ -870,7 +1051,7 @@
 
 def splits_well(mesh):
     n = mesh.shape["sp"]
-    return n > 2 and n <= 4 and mesh.shape["fs"] == 4 and mesh.shape["tp"] == 2
+    return n == 4 and mesh.shape["fs"] == 4 and mesh.shape["tp"] == 2
 
 
 def shards(*arrays):

time: 109 us -> 97 us (0.89)
  the two profiles are of different devices: /device:TPU:0 before, /device:TPU:12 now
where the time goes in v1:
time: 97 us; the launch traced here: 96.8 us
  Pallas kernels  95.1 us (98%)
  local copies, waits for them, and re-layouts  1.72 us (2%)
    pallas_call x1, Pallas kernels, split_shards(): pl.pallas_call(functools.partial(layer_kernel, n, parts, orders(n)), out_...  95.1 us

profile of v1, /device:TPU:12, one launch (start us, length us, event | category | flops | bytes accessed | tf_op | source)
XLA Modules:
  0.0 96.8 jit_solution(4908842429877019277)
XLA Ops:
  0.0 95.1 %whole_layer.1 = bf16[80,2048]{1,0:T(8,128)(2,1)} custom-call(bf16[1,160,1024]{2,1,0:T(8,128)(2,1)} %tok_in.1, f32[1,2048]{1,0:T(1,128)} %bitcast.7, f32[1,512]{1,0:T(1,128)} %bitcast.9, f32[1,1024]{1,0:T(1,128)} %bitcast.8, f32[3,512]{1,0:T(4,128)} %taps_in.1, bf16[128,512]{1,0:T(8,128)(2,1)} %cb.1, bf16[128,512]{1,0:T(8,128)(2,1)} %cc.1, ...), custom_call_target="tpu_custom_call" | custom-call | tf_op jit(solution)/shard_map/whole_layer/pallas_call | solution.py:985
  95.1 1.7 %copy.18 = bf16[1,80,2048]{2,1,0:T(8,128)(2,1)} copy(bf16[1,80,2048]{2,1,0:T(8,128)(2,1)} %bitcast.5) | data formatting | bytes 655360

commit v2 on v1

--- a/solution.py
+++ b/solution.py
@@ -269,19 +269,43 @@
 
 
 def orders(n):
-    arrival, compute, passing = [], [], []
+    columns = sorted(range(n), key=lambda g: (max(g, n - 1 - g), g))
+    arrival, steps, passes = [], [], []
+    slots = {}
+    for z in (0, n - 1):
+        by = [abs(z - d) for d in range(n)]
+        g = columns
+        sent = [(by[d], g[k]) for d, k in ((1, 0), (1, 1), (2, 0), (2, 1), (1, 2), (3, 0), (3, 1), (3, 2), (3, 3), (2, 2), (2, 3), (1, 3))]
+        slots[z] = sent
     for z in range(n):
-        first = z + 1 if z < n - 1 else z - 1
-        far = sorted((d for d in range(n) if d != z), key=lambda d: (-abs(d - z), min(d, n - 1 - d)))
-        arrival.append(sorted(range(n), key=lambda d: (abs(d - z), d)))
-        compute.append([first] + sorted((d for d in far if d != first), key=lambda d: -abs(d - z)) + [z])
-        passing.append(far)
-    return arrival, compute, passing
+        end = 0 if 2 * z < n else n - 1
+        near = sorted((d for d in range(n) if d != z), key=lambda d: (abs(d - z), abs(d - end)))
+        arrival.append([z] + near)
+        if z == end:
+            steps.append(slots[z] + [(z, g) for g in columns])
+            passes.append([(z, 0)])
+            continue
+        opposite = n - 1 - end
+        seen = [(i, step) for i, step in enumerate(slots[end]) if step[0] not in (z, end)]
+        seen += [(i + 2.2, step) for i, step in enumerate(slots[opposite]) if step[0] == end]
+        passes.append([step for _, step in sorted(seen)])
+        steps.append([(d, g) for g in columns for d in near + [z]])
+    first_column, first_block = [], []
+    for listed in steps:
+        blocks_seen, columns_seen, at_column, at_block = set(), set(), [], []
+        for d, g in listed:
+            at_column.append(n if g in columns_seen else columns.index(g))
+            at_block.append(0 if d in blocks_seen else 1)
+            columns_seen.add(g)
+            blocks_seen.add(d)
+        first_column.append(at_column)
+        first_block.append(at_block)
+    split = lambda table, i: [[pair[i] for pair in row] for row in table]
+    return arrival, columns, split(steps, 0), split(steps, 1), first_column, first_block, split(passes, 0), split(passes, 1)
 
 
 def layer_kernel(
     n,
-    parts,
     order,
     tok_in,
     mix_gain_in,
@@ -327,7 +351,6 @@
     moving,
     fetched,
     wsem,
-    fsem,
     lsem,
     tsem,
     psem,
@@ -335,12 +358,17 @@
     ssem,
     pairsem,
     zsem,
+    gone,
+    mix,
+    summed_out,
 ):
     here = Place()
     z, f, c = here.z, here.f, here.c
     fx, fy = flip(f, 1), flip(f, 2)
     other = 1 - c
     is_end = (z == 0) | (z == n - 1)
+    near = jnp.where(2 * z < n, -1, 1)
+    sides = (near, -near)
     rows = cb.shape[0]
     members = (cb, cc, cv, qw, qr)
     widths = [m.shape[1] // n for m in members]
@@ -367,11 +395,21 @@
     def arrive_at(t):
         return chosen(order[0], t)
 
-    def turn_of(t):
-        return chosen(order[1], t)
-
-    def pass_of(t):
-        return chosen(order[2], t)
+    def packed(table, bits):
+        words = []
+        for row in table:
+            word = sum(v << (bits * t) for t, v in enumerate(row))
+            words.append(word - (1 << 32) if word >= 1 << 31 else word)
+        mine = jnp.int32(words[0])
+        for zz in range(1, n):
+            mine = jnp.where(z == zz, jnp.int32(words[zz]), mine)
+        return lambda t: jnp.right_shift(mine, bits * t) & ((1 << bits) - 1)
+
+    step_block, step_column = packed(order[2], 2), packed(order[3], 2)
+    column_opens = packed([[int(k < n) for k in row] for row in order[4]], 1)
+    block_opens = packed(order[5], 1)
+    pass_block, pass_column = packed(order[6], 2), packed(order[7], 2)
+    column_at = packed([order[1]] * n, 2)
 
     greet(
         [here.to(z=lax.rem(z + j, n)) for j in range(1, n)]
@@ -407,8 +445,8 @@
 
     def send_own(kind):
         for src, dst in pieces(kind, z):
-            remote(src, dst, wsem.at[kind, 2, z], wsem.at[kind, 3, z], here.to(f=fx)).start()
-            remote(src, dst, wsem.at[kind, 4, z], wsem.at[kind, 5, z], here.to(f=fy)).start()
+            remote(src, dst, gone.at[kind], wsem.at[kind, 1, z], here.to(f=fx)).start()
+            remote(src, dst, gone.at[kind], wsem.at[kind, 2, z], here.to(f=fy)).start()
             pltpu.make_async_copy(src, dst, lsem.at[kind]).start()
 
     def can(sign):
@@ -424,7 +462,7 @@
         return (dest > 0) & (dest < n - 1)
 
     def serves(sign):
-        return z + sign == (n - 1 if sign > 0 else 0)
+        return z + sign == jnp.where(sign > 0, n - 1, 0)
 
     def send_z(kind, distance, sign):
         dest = z + sign * distance
@@ -432,15 +470,15 @@
         @pl.when(reached(distance, sign) if kind == 2 else within(dest))
         def _():
             for src, dst in pieces(kind, dest):
-                remote(src, dst, wsem.at[kind, 0, dest], wsem.at[kind, 1, z], here.to(z=dest)).start()
+                remote(src, dst, gone.at[kind], wsem.at[kind, 0, z], here.to(z=dest)).start()
 
     def plane_copy(kind, zs, role, fs, to):
         block = blocks[kind](zs, fs)
-        return remote(block, block, wsem.at[kind, role, zs], wsem.at[kind, role + 1, zs], here.to(f=to))
+        return remote(block, block, gone.at[kind], wsem.at[kind, role, zs], here.to(f=to))
 
     def end_copy(zs, sign):
         block = low_block(zs, f)
-        return remote(block, block, fsem.at[zs], wsem.at[2, 1, zs], here.to(z=z + sign))
+        return remote(block, block, gone.at[2], wsem.at[2, 0, zs], here.to(z=z + sign))
 
     def relay_z(kind, distance, sign):
         zs = z + sign * distance
@@ -448,44 +486,46 @@
         @pl.when(within(zs))
         def _():
             block = blocks[kind](zs, f)
-            remote(block, block, wsem.at[kind, 0, zs], wsem.at[kind, 1, zs], here.to(z=zs)).wait_recv()
+            remote(block, block, gone.at[kind], wsem.at[kind, 0, zs], here.to(z=zs)).wait_recv()
             if kind == 2:
                 pl.when(serves(-sign))(lambda: end_copy(zs, -sign).start())
-            plane_copy(kind, zs, 2, f, fx).start()
-            plane_copy(kind, zs, 4, f, fy).start()
+            plane_copy(kind, zs, 1, f, fx).start()
+            plane_copy(kind, zs, 2, f, fy).start()
 
     def relay_plane(kind, zs):
-        plane_copy(kind, zs, 2, fx, fx).wait_recv()
+        plane_copy(kind, zs, 1, fx, fx).wait_recv()
 
         @pl.when(zs % 2 == 0)
         def _():
-            plane_copy(kind, zs, 6, fx, fy).start()
-
-        plane_copy(kind, zs, 4, fy, fy).wait_recv()
+            plane_copy(kind, zs, 3, fx, fy).start()
+
+        plane_copy(kind, zs, 2, fy, fy).wait_recv()
 
         @pl.when(zs % 2 == 1)
         def _():
-            plane_copy(kind, zs, 6, fy, fx).start()
+            plane_copy(kind, zs, 3, fy, fx).start()
 
     def relay_done(kind, zs):
-        plane_copy(kind, zs, 6, flip(fx, 2), fx).wait_recv()
+        plane_copy(kind, zs, 3, flip(fx, 2), fx).wait_recv()
 
     def tok_block(owner, zs, i):
         return tok.at[owner, pl.ds(pl.multiple_of(zs * tr + i * hr, hr), hr), :]
 
+    def half_at(sign, i):
+        return jnp.where(sign > 0, 1 - i, i)
+
     own_tok = [tok_in.at[0, i * hr : (i + 1) * hr, :] for i in range(2)]
 
     def tok_copy(zs, sign, hop, i, src=None):
-        d = (sign + 1) // 2
         block = tok_block(c, zs, i)
         return remote(
-            block if src is None else src, block, tsem.at[d, 0, hop, i], tsem.at[d, 1, hop, i], here.to(z=z + sign)
+            block if src is None else src, block, gone.at[3], tsem.at[zs, i], here.to(z=z + sign)
         )
 
     def partner_copy(zs, owner, i, src=None):
         block = tok_block(owner, zs, i)
         return remote(
-            block if src is None else src, block, psem.at[0, zs, i], psem.at[1, zs, i], here.to(c=other)
+            block if src is None else src, block, gone.at[4], psem.at[zs, i], here.to(c=other)
         )
 
     def own_copy(i):
@@ -516,24 +556,31 @@
     for i in range(2):
         partner_copy(z, c, i, own_tok[i]).start()
         own_copy(i).start()
-    for kind in (0, 1):
-        send_own(kind)
-
-    def send_inward(kind, distance, sign):
-        pl.when(jnp.logical_not(serves(sign)))(lambda: send_z(kind, distance, sign))
-
-    def send_outward(kind, sign):
-        pl.when(serves(sign))(lambda: send_z(kind, 1, sign))
-
-    def send_tok(sign):
-        for i in range(2):
-            pl.when(can(sign))(lambda i=i: tok_copy(z, sign, 0, i, own_tok[i]).start())
-
-    for kind in (0, 1):
+    send_own(0)
+    middle = jnp.logical_not(is_end)
+
+    def send_far_first(kind):
+        for distance in (2, 1):
+            for sign in (-1, 1):
+                send_z(kind, distance, sign)
+
+    def send_near_first(kind):
         for distance, sign in steps:
-            send_inward(kind, distance, sign)
-    for sign in (-1, 1):
-        pl.when(jnp.logical_not(serves(sign)))(lambda sign=sign: send_tok(sign))
+            send_z(kind, distance, sign)
+
+    def send_toks():
+        for sign in (-1, 1):
+            for i in (1, 0) if sign > 0 else (0, 1):
+                pl.when(can(sign))(lambda sign=sign, i=i: tok_copy(z, sign, 0, i, own_tok[i]).start())
+
+    pl.when(middle)(lambda: send_far_first(0))
+
+    @pl.when(is_end)
+    def _():
+        send_near_first(0)
+        send_toks()
+
+
     for i, (src, dst) in enumerate(small):
         pltpu.make_async_copy(src, dst, ssem.at[i]).start()
 
@@ -542,14 +589,15 @@
 
         @pl.when(within(zs))
         def _():
-            tok_copy(zs, -sign, distance - 1, i).wait_recv()
+            half = half_at(-sign, i)
+            tok_copy(zs, -sign, distance - 1, half).wait_recv()
             if distance < n - 1:
-                pl.when(can(-sign))(lambda: tok_copy(zs, -sign, distance, i).start())
-            partner_copy(zs, c, i).start()
-
-    def relay_toks(distance):
-        for i in range(2):
-            for sign in (-1, 1):
+                pl.when(can(-sign))(lambda: tok_copy(zs, -sign, distance, half).start())
+            partner_copy(zs, c, half).start()
+
+    def relay_toks(distance, sides=sides):
+        for sign in sides:
+            for i in range(2):
                 relay_tok(distance, sign, i)
 
     def each_zs(fn):
@@ -560,7 +608,7 @@
         lax.fori_loop(0, n, body, 0)
 
     def at_distance(distance, fn):
-        for sign in (-1, 1):
+        for sign in sides:
             zs = z + sign * distance
             pl.when(within(zs))(lambda zs=zs: fn(zs))
 
@@ -582,33 +630,35 @@
     prod[0:head_rows, :] = jnp.zeros((head_rows, channels), prod.dtype)
 
     def rotated(x, at):
-        swapped = jnp.where(
-            first_half, pltpu.roll(x, rot_w - ROPE // 2, 1), pltpu.roll(x, ROPE // 2, 1)
-        )
+        low_half = (lax.broadcasted_iota(jnp.int32, x.shape, 1) % ROPE) < ROPE // 2
+        swapped = jnp.where(low_half, pltpu.roll(x, rot_w - ROPE // 2, 1), pltpu.roll(x, ROPE // 2, 1))
         return (x * cosine[at, :] + swapped * sine[at, :]).astype(jnp.bfloat16)
 
     for i, (src, dst) in enumerate(small):
         pltpu.make_async_copy(src, dst, ssem.at[i]).wait()
     wide = tok.shape[2]
 
+    def half_rows(zs, i):
+        return pl.ds(pl.multiple_of(zs * tr + i * hr, hr), hr)
+
+    def norm_half(zs, i):
+        partner_copy(zs, other, i).wait_recv()
+        at = half_rows(zs, i)
+        first = tok[0, at, :].astype(jnp.float32)
+        second = tok[1, at, :].astype(jnp.float32)
+        mean = (
+            jnp.sum(first * first, axis=-1, keepdims=True) + jnp.sum(second * second, axis=-1, keepdims=True)
+        ) / (2 * wide)
+        scale = lax.rsqrt(mean + norm_epsilon)
+        normed[at, 0:wide] = (first * scale * gain[0:1, 0:wide]).astype(jnp.bfloat16)
+        normed[at, wide : 2 * wide] = (second * scale * gain[0:1, wide : 2 * wide]).astype(jnp.bfloat16)
+
     def norm_block(zs):
-        for i in range(2):
-            partner_copy(zs, other, i).wait_recv()
-
-        def norm_chunk(i, carry):
-            at = pl.ds(pl.multiple_of(zs * tr + i * hr, hr), hr)
-            first = tok[0, at, :].astype(jnp.float32)
-            second = tok[1, at, :].astype(jnp.float32)
-            mean = (
-                jnp.sum(first * first, axis=-1, keepdims=True)
-                + jnp.sum(second * second, axis=-1, keepdims=True)
-            ) / (2 * wide)
-            scale = lax.rsqrt(mean + norm_epsilon)
-            normed[at, 0:wide] = (first * scale * gain[0:1, 0:wide]).astype(jnp.bfloat16)
-            normed[at, wide : 2 * wide] = (second * scale * gain[0:1, wide : 2 * wide]).astype(jnp.bfloat16)
+        def body(i, carry):
+            norm_half(zs, i)
             return carry
 
-        lax.fori_loop(0, 2, norm_chunk, 0)
+        lax.fori_loop(0, 2, body, 0)
 
     def rows_of(zs):
         return pl.ds(pl.multiple_of(zs * tr, tr), tr)
@@ -623,22 +673,22 @@
 
     def lat_copy(k, dest):
         block = shared[k](z, c)
-        return remote(block, block, latsem.at[k, 0, dest], latsem.at[k, 1, z], here.to(z=dest))
+        return remote(block, block, gone.at[5 + k], latsem.at[k, 0, z], here.to(z=dest))
 
     def lat_arrival(k, zs):
         block = shared[k](zs, c)
-        return remote(block, block, latsem.at[k, 0, zs], latsem.at[k, 1, zs], here.to(z=zs))
+        return remote(block, block, gone.at[5 + k], latsem.at[k, 0, zs], here.to(z=zs))
 
     def lat_forward(k, zs, sign):
         block = shared[k](zs, c)
-        return remote(block, block, latsem.at[k, 4, zs], latsem.at[k, 1, zs], here.to(z=z + sign))
+        return remote(block, block, gone.at[5 + k], latsem.at[k, 0, zs], here.to(z=z + sign))
 
     def lat_partner(k, zs, owner):
         block = shared[k](zs, owner)
-        return remote(block, block, latsem.at[k, 2, zs], latsem.at[k, 3, zs], here.to(c=other))
-
-    def relay_lat(distance):
-        for sign in (-1, 1):
+        return remote(block, block, gone.at[5 + k], latsem.at[k, 1, zs], here.to(c=other))
+
+    def relay_lat(distance, sides=sides):
+        for sign in sides:
             zs = z + sign * distance
 
             @pl.when(within(zs))
@@ -666,67 +716,117 @@
         for kind in (0, 1):
             relay_plane(kind, zs)
 
-    for sign in (-1, 1):
-        relay_z(2, 1, sign)
+    def relay_all_z(kind, distance):
+        for sign in sides:
+            relay_z(kind, distance, sign)
+
+    def diagonals(kind, distance):
+        at_distance(distance, lambda zs: relay_plane(kind, zs))
+
+    def share_latents():
+        pltpu.make_async_copy(low_block(z, f), low_block(z, f), lsem.at[2]).wait()
+        each_zs(lambda zs: relay_done(2, zs))
+        own_latents()
+        for distance, sign in steps:
+            dest = z + sign * distance
+
+            @pl.when(reached(distance, sign))
+            def _(dest=dest):
+                for k in range(2):
+                    lat_copy(k, dest).start()
+
+        lat_partner(0, z, c).start()
+
+    relay_all_z(2, 1)
     relay_plane(2, z)
-    pl.when(jnp.logical_not(is_end))(lambda: [relay_z(2, 2, sign) for sign in (-1, 1)] and None)
-    for sign in (-1, 1):
-        for kind in (0, 1):
-            send_outward(kind, sign)
-        pl.when(serves(sign))(lambda sign=sign: send_tok(sign))
     for i in range(2):
         own_copy(i).wait()
     norm_block(z)
-    pl.when(is_end)(lambda: [relay_z(2, 2, sign) for sign in (-1, 1)] and None)
-    for distance in range(3, n):
-        for sign in (-1, 1):
-            relay_z(2, distance, sign)
-    relay_plane(0, z)
-    relay_plane(1, z)
-    for sign in (-1, 1):
-        relay_z(0, 1, sign)
-    for distance in range(1, n):
-        at_distance(distance, lambda zs: relay_plane(2, zs))
-    for sign in (-1, 1):
-        relay_z(0, 2, sign)
-    at_distance(1, lambda zs: relay_plane(0, zs))
-    pltpu.make_async_copy(low_block(z, f), low_block(z, f), lsem.at[2]).wait()
-    each_zs(lambda zs: relay_done(2, zs))
-    own_latents()
-    for distance, sign in steps:
-        dest = z + sign * distance
-
-        @pl.when(reached(distance, sign))
-        def _(dest=dest):
-            for k in range(2):
-                lat_copy(k, dest).start()
-
-    lat_partner(0, z, c).start()
-    for distance in range(3, n):
-        for sign in (-1, 1):
-            relay_z(0, distance, sign)
-    for sign in (-1, 1):
-        relay_z(1, 1, sign)
-    for sign in (-1, 1):
-        relay_z(1, 2, sign)
-    at_distance(2, lambda zs: relay_plane(0, zs))
-    for distance in range(3, n):
-        for sign in (-1, 1):
-            relay_z(1, distance, sign)
-    relay_toks(1)
-    at_distance(1, lambda zs: relay_plane(1, zs))
+
+    @pl.when(is_end)
+    def _():
+        relay_plane(0, z)
+        send_own(1)
+        for distance in range(2, n):
+            relay_all_z(2, distance)
+        relay_all_z(0, 1)
+        for distance in range(1, n):
+            diagonals(2, distance)
+        relay_all_z(0, 2)
+        relay_all_z(0, 3)
+        share_latents()
+        diagonals(0, 1)
+        send_near_first(1)
+        diagonals(0, 2)
+        diagonals(0, 3)
+        relay_lat(1)
+        relay_toks(1)
+
+    @pl.when(middle)
+    def _():
+        relay_all_z(2, 2)
+        relay_plane(0, z)
+        diagonals(2, 1)
+        diagonals(2, 2)
+        relay_z(0, 1, near)
+        relay_all_z(0, 2)
+        share_latents()
+        send_toks()
+        send_far_first(1)
+        relay_plane(0, z + near)
+        relay_z(0, 1, -near)
+        diagonals(0, 2)
+        relay_lat(1, sides[1:])
+        relay_toks(1, sides[:1])
+        send_own(1)
+        relay_plane(0, z - near)
+        relay_lat(1, sides[:1])
+        relay_lat(2)
+        relay_toks(1, sides[1:])
+
+    pltpu.make_async_copy(in_block(z, f), in_block(z, f), lsem.at[0]).wait()
+    each_zs(lambda zs: relay_done(0, zs))
+
+    @pl.when(is_end)
+    def _():
+        pl.when(z == 0)(lambda: relay_all_z(1, 1))
+        relay_all_z(1, 2)
+        pl.when(z != 0)(lambda: relay_all_z(1, 1))
+
+    pl.when(middle)(lambda: relay_z(1, 1, -near))
     norm_block(arrive_at(1))
-    relay_lat(1)
-    for distance in range(3, n):
-        at_distance(distance, lambda zs: relay_plane(0, zs))
-    at_distance(2, lambda zs: relay_plane(1, zs))
-    relay_lat(2)
-    relay_toks(2)
-    for distance in range(3, n):
-        at_distance(distance, lambda zs: relay_plane(1, zs))
-        relay_lat(distance)
-    for t in range(2, n - 1):
-        norm_block(arrive_at(t))
+
+    def project_rows(first_row, count):
+        at = pl.ds(pl.multiple_of(first_row, hr), count)
+        joined = jnp.dot(normed[at, :], win[...], preferred_element_type=jnp.float32)
+        gates = joined[:, channels : 3 * channels].astype(jnp.bfloat16).astype(jnp.float32)
+        gate[at, :] = joined[:, 0:channels].astype(jnp.bfloat16)
+        below = pl.ds(pl.multiple_of(first_row + head_rows, head_rows), count)
+        prod[below, :] = (gates[:, 0:channels] * gates[:, channels : 2 * channels]).astype(jnp.bfloat16)
+        start = 3 * channels
+        q_nope[at, :] = joined[:, start : start + heads * NOPE].astype(jnp.bfloat16)
+        q_rot[at, :] = rotated(joined[:, start + heads * NOPE :], at)
+
+    def project_half(zs, i):
+        project_rows(zs * tr + i * hr, hr)
+
+    def project_arrived(t, carry):
+        project_rows(arrive_at(t) * tr, tr)
+        return carry
+
+    lax.fori_loop(0, 2, project_arrived, 0)
+
+    @pl.when(is_end)
+    def _():
+        relay_lat(2)
+        relay_lat(3)
+        relay_all_z(1, 3)
+
+    @pl.when(middle)
+    def _():
+        relay_z(1, 1, near)
+        relay_all_z(1, 2)
+
 
     def lat_waits(zs):
         lat_partner(0, zs, other).wait_recv()
@@ -747,20 +847,8 @@
         return carry
 
     lax.fori_loop(0, n, expand, 0)
-    for kind in (0, 1):
-        pltpu.make_async_copy(blocks[kind](z, f), blocks[kind](z, f), lsem.at[kind]).wait()
-    each_zs(lambda zs: [relay_done(kind, zs) for kind in (0, 1)] and None)
-
-    def project(zs):
-        at = rows_of(zs)
-        joined = jnp.dot(normed[at, :], win[...], preferred_element_type=jnp.float32)
-        gates = joined[:, channels : 3 * channels].astype(jnp.bfloat16).astype(jnp.float32)
-        gate[at, :] = joined[:, 0:channels].astype(jnp.bfloat16)
-        below = pl.ds(pl.multiple_of(zs * tr + head_rows, head_rows), tr)
-        prod[below, :] = (gates[:, 0:channels] * gates[:, channels : 2 * channels]).astype(jnp.bfloat16)
-        start = 3 * channels
-        q_nope[at, :] = joined[:, start : start + heads * NOPE].astype(jnp.bfloat16)
-        q_rot[at, :] = rotated(joined[:, start + heads * NOPE :], at)
+    relay_plane(1, order[1][0])
+    pl.when(middle)(lambda: relay_toks(2))
 
     shift = SEG.bit_length() - 1
     row_index = lax.broadcasted_iota(jnp.int32, (tr, length), 0)
@@ -768,7 +856,7 @@
     own_lanes = lane // ROPE
     own_channels = pl.ds(pl.multiple_of(z * channels, channels), channels)
 
-    def block_output(dest):
+    def features(dest):
         at = rows_of(dest)
         allowed = key_segment <= jnp.right_shift(row_index + dest * tr, shift)
         padded = prod[pl.ds(pl.multiple_of(dest * tr, head_rows), tr + head_rows), :].astype(jnp.float32)
@@ -804,148 +892,187 @@
             mean = jnp.mean(head_out * head_out, axis=-1, keepdims=True)
             gained = head_out * lax.rsqrt(mean + norm_epsilon) * head_gain[0:1, h * VD : (h + 1) * VD]
             outputs.append(gained.astype(jnp.bfloat16))
-        mixed = jnp.concatenate(outputs, axis=1)
-        part[dest] = jnp.dot(mixed, wout[...], preferred_element_type=jnp.float32).astype(jnp.bfloat16)
-
-    def part_rows(dest, core):
-        return part.at[dest, pl.ds(pl.multiple_of(core * share, share), share), :]
-
-    def pair_copy(dest):
+        mix[dest] = jnp.concatenate(outputs, axis=1)
+
+    piece_w = wout.shape[1] // n
+
+    def cut(g):
+        return pl.ds(pl.multiple_of(g * piece_w, piece_w), piece_w)
+
+    def own_rows():
+        return pl.ds(pl.multiple_of(c * share, share), share)
+
+    def pair_copy(dest, g):
+        theirs = pl.ds(pl.multiple_of(other * share, share), share)
         return remote(
-            part_rows(dest, other), pair.at[dest], pairsem.at[0, dest], pairsem.at[1, dest], here.to(c=other)
+            part.at[dest, theirs, cut(g)],
+            pair.at[dest, :, cut(g)],
+            gone.at[7],
+            pairsem.at[dest, g],
+            here.to(c=other),
         )
 
-    piece_w = out.shape[1] // parts
-
-    def cut(g):
-        return slice(g * piece_w, (g + 1) * piece_w)
-
-    def line_copy(d, dest, g):
+    def line_copy(d, dest, g, target):
+        row = jnp.where((dest == target) & (d == 1), n, dest)
         return remote(
             moving.at[dest, :, cut(g)],
             fetched.at[d, dest, :, cut(g)],
-            zsem.at[d, 0, dest, g],
-            zsem.at[d, 1, dest, g],
+            gone.at[8],
+            zsem.at[row, g],
             here.to(z=z + 2 * d - 1),
         )
 
+    def line_send(d, dest, g):
+        line_copy(d, dest, g, z + 2 * d - 1).start()
+
     def summed(dest, g):
-        kept = part[dest, pl.ds(pl.multiple_of(c * share, share), share), cut(g)]
+        kept = part[dest, own_rows(), cut(g)]
         return kept.astype(jnp.float32) + pair[dest, :, cut(g)].astype(jnp.float32)
 
     def toward(dest):
         return jnp.where(dest > z, 1, 0)
 
-    def pass_first(dest):
-        pair_copy(dest).wait_recv()
-        for g in range(parts):
-            moving[dest, :, cut(g)] = summed(dest, g).astype(jnp.bfloat16)
-            line_copy(toward(dest), dest, g).start()
-
-    def pass_on(dest):
+    def pass_first(dest, g):
+        pair_copy(dest, g).wait_recv()
+        moving[dest, :, cut(g)] = summed(dest, g).astype(jnp.bfloat16)
+        line_send(toward(dest), dest, g)
+
+    def pass_on(dest, g):
         d = toward(dest)
-        pair_copy(dest).wait_recv()
-        for g in range(parts):
-            line_copy(d, dest, g).wait_recv()
-            moving[dest, :, cut(g)] = (
-                summed(dest, g) + fetched[d, dest, :, cut(g)].astype(jnp.float32)
-            ).astype(jnp.bfloat16)
-            line_copy(d, dest, g).start()
-
-    def project_arrived(t, carry):
-        project(arrive_at(t))
+        pair_copy(dest, g).wait_recv()
+        line_copy(d, dest, g, z).wait_recv()
+        moving[dest, :, cut(g)] = (
+            summed(dest, g) + fetched[d, dest, :, cut(g)].astype(jnp.float32)
+        ).astype(jnp.bfloat16)
+        line_send(d, dest, g)
+
+    def process_half(zs, i):
+        norm_half(zs, i)
+        project_half(zs, i)
+
+    @pl.when(middle)
+    def _():
+        def rest(t, carry):
+            norm_block(arrive_at(t))
+            return project_arrived(t, carry)
+
+        lax.fori_loop(2, n, rest, 0)
+
+    half_first = half_at(-sides[1], 0)
+    half_last = 1 - half_first
+
+    @pl.when(is_end)
+    def _():
+        relay_tok(2, sides[1], 0)
+        process_half(arrive_at(2), half_first)
+
+    relay_plane(1, order[1][1])
+
+
+    second_block, third_block = [i for i, opens in enumerate(order[5][0]) if opens][1:3]
+
+    def step(i, carry):
+        dest, g = step_block(i), step_column(i)
+        before = jnp.maximum(i - 1, 0)
+
+        def pass_before():
+            pass_first(step_block(before), step_column(before))
+
+        pl.when(block_opens(i) == 1)(lambda: features(dest))
+
+        @pl.when(column_opens(i) == 1)
+        def _():
+            pl.when(g == z)(lambda: pltpu.make_async_copy(out_block(z, f), out_block(z, f), lsem.at[1]).wait())
+            relay_done(1, g)
+
+        part[dest, :, cut(g)] = jnp.dot(
+            mix[dest], wout[:, cut(g)], preferred_element_type=jnp.float32
+        ).astype(jnp.bfloat16)
+        pair_copy(dest, g).start()
+        pl.when(is_end & (i >= 1) & (i <= n * (n - 1)))(pass_before)
+        for k in range(2, n):
+            pl.when(i == k - 2)(lambda k=k: relay_plane(1, order[1][k]))
+
+        @pl.when(is_end)
+        def _():
+            @pl.when(i == 0)
+            def _():
+                relay_tok(2, sides[1], 1)
+                relay_tok(3, sides[1], 0)
+
+            pl.when(i == third_block - 3)(lambda: relay_tok(3, sides[1], 1))
+
+            @pl.when((i == 1) | (i == third_block - 2))
+            def _():
+                first = jnp.where(i == 1, 0, 2)
+
+                def late(t, carry):
+                    process_half(jnp.where(t == 0, arrive_at(2), arrive_at(3)), jnp.where(t == 1, half_first, half_last))
+                    return carry
+
+                lax.fori_loop(first, jnp.where(i == 1, 2, 3), late, 0)
+
         return carry
 
-    lax.fori_loop(0, n - 1, project_arrived, 0)
-
-    def turn(t, carry):
-        @pl.when(t == 1)
+    lax.fori_loop(0, n * n, step, 0)
+
+    @pl.when(middle)
+    def _():
+        def passing(i, carry):
+            pass_on(pass_block(i), pass_column(i))
+            return carry
+
+        lax.fori_loop(0, n * (n - 1), passing, 0)
+
+    low, high = z > 0, z < n - 1
+
+    def out_copy(g):
+        return pltpu.make_async_copy(summed_out.at[:, cut(g)], out.at[:, cut(g)], gone.at[9])
+
+    def finish(turn, carry):
+        g = column_at(turn)
+        pair_copy(z, g).wait_recv()
+        pl.when(low)(lambda: line_copy(1, z, g, z).wait_recv())
+        pl.when(high)(lambda: line_copy(0, z, g, z).wait_recv())
+
+        @pl.when(middle)
         def _():
-            pl.when(is_end)(lambda: pass_first(turn_of(0)))
-            for distance in range(3, n):
-                relay_toks(distance)
-            last = arrive_at(n - 1)
-            norm_block(last)
-            project(last)
-
-        dest = turn_of(t)
-        block_output(dest)
-        pair_copy(dest).start()
-        pl.when((t >= 2) & is_end)(lambda: pass_first(turn_of(t - 1)))
-        return carry
-
-    lax.fori_loop(0, n, turn, 0)
-
-    @pl.when(jnp.logical_not(is_end))
-    def _():
-        def passing(t, carry):
-            pass_on(pass_of(t))
-            return carry
-
-        lax.fori_loop(0, n - 1, passing, 0)
-
-    pair_copy(z).wait_recv()
-    low, high = z > 0, z < n - 1
-    for g in range(parts):
-        pl.when(low)(lambda: line_copy(1, z, g).wait_recv())
-        pl.when(high)(lambda: line_copy(0, z, g).wait_recv())
-
-        @pl.when(low & high)
-        def _():
-            out[:, cut(g)] = (
+            summed_out[:, cut(g)] = (
                 summed(z, g)
                 + fetched[1, z, :, cut(g)].astype(jnp.float32)
                 + fetched[0, z, :, cut(g)].astype(jnp.float32)
             ).astype(jnp.bfloat16)
 
-        @pl.when(jnp.logical_not(low & high))
+        @pl.when(is_end)
         def _():
             d = jnp.where(low, 1, 0)
-            out[:, cut(g)] = (summed(z, g) + fetched[d, z, :, cut(g)].astype(jnp.float32)).astype(jnp.bfloat16)
-
-    for j in range(1, n):
-        zs = lax.rem(z + j, n)
-        for kind in (0, 1):
-            block = blocks[kind](zs, f)
-            remote(block, block, wsem.at[kind, 0, zs], wsem.at[kind, 1, zs], here.to(z=zs)).wait_send()
-        for g in range(parts):
-            line_copy(toward(zs), zs, g).wait_send()
-        lat_partner(1, zs, c).wait_send()
-    for distance, sign in steps:
-        dest = z + sign * distance
-
-        @pl.when(reached(distance, sign))
-        def _(dest=dest):
-            block = low_block(dest, f)
-            remote(block, block, wsem.at[2, 0, dest], wsem.at[2, 1, dest], here.to(z=dest)).wait_send()
-            for k in range(2):
-                lat_copy(k, dest).wait_send()
-
-        @pl.when(within(dest) & serves(-sign))
-        def _(dest=dest, sign=sign):
-            end_copy(dest, -sign).wait_send()
-            for k in range(2):
-                lat_forward(k, dest, -sign).wait_send()
-
-    def sent(zs):
-        for kind in (0, 1, 2):
-            plane_copy(kind, zs, 2, f, fx).wait_send()
-            plane_copy(kind, zs, 4, f, fy).wait_send()
-            plane_copy(kind, zs, 6, fx, fy).wait_send()
-        for i in range(2):
-            partner_copy(zs, c, i).wait_send()
-        lat_partner(0, zs, c).wait_send()
-        pair_copy(zs).wait_send()
-
-    each_zs(sent)
-    for sign in (-1, 1):
-        for i in range(2):
-            pl.when(can(sign))(lambda sign=sign, i=i: tok_copy(z, sign, 0, i).wait_send())
-            for distance in range(1, n - 1):
-                zs = z - sign * distance
-                pl.when(within(zs) & can(sign))(
-                    lambda sign=sign, distance=distance, i=i: tok_copy(z, sign, distance, i).wait_send()
-                )
+            summed_out[:, cut(g)] = (
+                summed(z, g) + fetched[d, z, :, cut(g)].astype(jnp.float32)
+            ).astype(jnp.bfloat16)
+
+        out_copy(g).start()
+        return carry
+
+    lax.fori_loop(0, n, finish, 0)
+
+    def sent(sem, ref):
+        pltpu.make_async_copy(ref, ref, gone.at[sem]).wait()
+
+    def by_place(sem, at_ends, at_middle):
+        pl.when(is_end)(lambda: sent(sem, at_ends))
+        pl.when(middle)(lambda: sent(sem, at_middle))
+
+    whole = 4 * n - 1
+    sent(0, win.at[0 : whole * rows, :])
+    sent(1, wout.at[:, 0 : whole * out_cols])
+    by_place(2, wlat.at[0 : (3 * n + 2) * rows, :], wlat.at[0 : 4 * n * rows, :])
+    by_place(3, tok.at[:, 0:hr, :], tok.at[:, 0 : (n + 1) * hr, :])
+    sent(4, tok.at[0])
+    by_place(5, lat.at[:, 0 : 3 * tr, :], lat)
+    by_place(6, krot.at[0 : 5 * hr, :], krot.at[0 : 7 * hr, :])
+    sent(7, pair)
+    sent(8, moving.at[0 : n - 1])
+    sent(9, summed_out)
 
 
 def split_shards(
@@ -978,15 +1105,14 @@
     out_rows = (conv_out_weight.shape[0] + attn_out_weight.shape[0]) // n
     columns = attn_out_weight.shape[1] * n * 4
     share = tr // 2
-    parts = 4
     head_rows = 16
     bf16, f32 = jnp.bfloat16, jnp.float32
     dma = pltpu.SemaphoreType.DMA
     result = pl.pallas_call(
-        functools.partial(layer_kernel, n, parts, orders(n)),
+        functools.partial(layer_kernel, n, orders(n)),
         out_shape=jax.ShapeDtypeStruct((share, columns), bf16),
         in_specs=[pl.BlockSpec(memory_space=pltpu.HBM)] * 16,
-        out_specs=pl.BlockSpec(memory_space=pltpu.VMEM),
+        out_specs=pl.BlockSpec(memory_space=pltpu.HBM),
         scratch_shapes=[
             pltpu.VMEM((2, length, wide), bf16),
             pltpu.VMEM((length, features), bf16),
@@ -1014,15 +1140,17 @@
             pltpu.VMEM((n, share, columns), bf16),
             pltpu.VMEM((n, share, columns), bf16),
             pltpu.VMEM((2, n, share, columns), bf16),
-            dma((3, 8, n)),
-            dma((n,)),
+            dma((3, 4, n)),
             dma((5,)),
-            dma((2, 2, n, 2)),
-            dma((2, n, 2)),
-            dma((2, 5, n)),
+            dma((n, 2)),
+            dma((n, 2)),
+            dma((2, 2, n)),
             dma((8,)),
-            dma((2, n)),
-            dma((2, 2, n, parts)),
+            dma((n, n)),
+            dma((n + 1, n)),
+            dma((10,)),
+            pltpu.VMEM((n, tr, out_rows), bf16),
+            pltpu.VMEM((share, columns), bf16),
         ],
         compiler_params=pltpu.CompilerParams(
             collective_id=0, has_side_effects=True, vmem_limit_bytes=60 * 1024 * 1024

time: 97 us -> 89.8 us (0.926)
  the two profiles are of different devices: /device:TPU:12 before, /device:TPU:0 now
where the time goes in v2:
time: 89.8 us; the launch traced here: 89.6 us
  Pallas kernels  87.9 us (98%)
  local copies, waits for them, and re-layouts  1.72 us (2%)
    pallas_call x1, Pallas kernels, split_shards(): pl.pallas_call(functools.partial(layer_kernel, n, orders(n)), out_shape=j...  87.9 us

profile of v2, /device:TPU:0, one launch (start us, length us, event | category | flops | bytes accessed | tf_op | source)
XLA Modules:
  0.0 89.6 jit_solution(1322843444673178418)
XLA Ops:
  0.0 87.9 %whole_layer.1 = bf16[80,2048]{1,0:T(8,128)(2,1)} custom-call(bf16[1,160,1024]{2,1,0:T(8,128)(2,1)} %tok_in.1, f32[1,2048]{1,0:T(1,128)} %bitcast.7, f32[1,512]{1,0:T(1,128)} %bitcast.9, f32[1,1024]{1,0:T(1,128)} %bitcast.8, f32[3,512]{1,0:T(4,128)} %taps_in.1, bf16[128,512]{1,0:T(8,128)(2,1)} %cb.1, bf16[128,512]{1,0:T(8,128)(2,1)} %cc.1, ...), custom_call_target="tpu_custom_call" | custom-call | tf_op jit(solution)/shard_map/whole_layer/pallas_call | solution.py:1111
  87.9 1.7 %copy.18 = bf16[1,80,2048]{2,1,0:T(8,128)(2,1)} copy(bf16[1,80,2048]{2,1,0:T(8,128)(2,1)} %bitcast.5) | data formatting | bytes 655360

commit v3 on v2

--- a/solution.py
+++ b/solution.py
@@ -360,7 +360,6 @@
     zsem,
     gone,
     mix,
-    summed_out,
 ):
     here = Place()
     z, f, c = here.z, here.f, here.c
@@ -820,12 +819,6 @@
     def _():
         relay_lat(2)
         relay_lat(3)
-        relay_all_z(1, 3)
-
-    @pl.when(middle)
-    def _():
-        relay_z(1, 1, near)
-        relay_all_z(1, 2)
 
 
     def lat_waits(zs):
@@ -848,7 +841,14 @@
 
     lax.fori_loop(0, n, expand, 0)
     relay_plane(1, order[1][0])
-    pl.when(middle)(lambda: relay_toks(2))
+    pl.when(is_end)(lambda: relay_all_z(1, 3))
+
+    @pl.when(middle)
+    def _():
+        relay_z(1, 1, near)
+        relay_all_z(1, 2)
+        relay_toks(2)
+
 
     shift = SEG.bit_length() - 1
     row_index = lax.broadcasted_iota(jnp.int32, (tr, length), 0)
@@ -964,6 +964,7 @@
     @pl.when(is_end)
     def _():
         relay_tok(2, sides[1], 0)
+        relay_tok(2, sides[1], 1)
         process_half(arrive_at(2), half_first)
 
     relay_plane(1, order[1][1])
@@ -978,7 +979,11 @@
         def pass_before():
             pass_first(step_block(before), step_column(before))
 
+        opens = (block_opens(i) == 1) | (column_opens(i) == 1)
+        passes = is_end & (i >= 1) & (i <= n * (n - 1))
+        pl.when(passes & opens)(pass_before)
         pl.when(block_opens(i) == 1)(lambda: features(dest))
+        pl.when(is_end & (i == 0))(lambda: process_half(arrive_at(2), half_last))
 
         @pl.when(column_opens(i) == 1)
         def _():
@@ -989,28 +994,18 @@
             mix[dest], wout[:, cut(g)], preferred_element_type=jnp.float32
         ).astype(jnp.bfloat16)
         pair_copy(dest, g).start()
-        pl.when(is_end & (i >= 1) & (i <= n * (n - 1)))(pass_before)
+        pl.when(passes & jnp.logical_not(opens))(pass_before)
         for k in range(2, n):
             pl.when(i == k - 2)(lambda k=k: relay_plane(1, order[1][k]))
 
         @pl.when(is_end)
         def _():
-            @pl.when(i == 0)
-            def _():
-                relay_tok(2, sides[1], 1)
-                relay_tok(3, sides[1], 0)
-
+            pl.when(i == 0)(lambda: relay_tok(3, sides[1], 0))
             pl.when(i == third_block - 3)(lambda: relay_tok(3, sides[1], 1))
 
             @pl.when((i == 1) | (i == third_block - 2))
             def _():
-                first = jnp.where(i == 1, 0, 2)
-
-                def late(t, carry):
-                    process_half(jnp.where(t == 0, arrive_at(2), arrive_at(3)), jnp.where(t == 1, half_first, half_last))
-                    return carry
-
-                lax.fori_loop(first, jnp.where(i == 1, 2, 3), late, 0)
+                process_half(arrive_at(3), jnp.where(i == 1, half_first, half_last))
 
         return carry
 
@@ -1026,9 +1021,6 @@
 
     low, high = z > 0, z < n - 1
 
-    def out_copy(g):
-        return pltpu.make_async_copy(summed_out.at[:, cut(g)], out.at[:, cut(g)], gone.at[9])
-
     def finish(turn, carry):
         g = column_at(turn)
         pair_copy(z, g).wait_recv()
@@ -1037,7 +1029,7 @@
 
         @pl.when(middle)
         def _():
-            summed_out[:, cut(g)] = (
+            out[:, cut(g)] = (
                 summed(z, g)
                 + fetched[1, z, :, cut(g)].astype(jnp.float32)
                 + fetched[0, z, :, cut(g)].astype(jnp.float32)
@@ -1046,11 +1038,10 @@
         @pl.when(is_end)
         def _():
             d = jnp.where(low, 1, 0)
-            summed_out[:, cut(g)] = (
+            out[:, cut(g)] = (
                 summed(z, g) + fetched[d, z, :, cut(g)].astype(jnp.float32)
             ).astype(jnp.bfloat16)
 
-        out_copy(g).start()
         return carry
 
     lax.fori_loop(0, n, finish, 0)
@@ -1072,7 +1063,6 @@
     by_place(6, krot.at[0 : 5 * hr, :], krot.at[0 : 7 * hr, :])
     sent(7, pair)
     sent(8, moving.at[0 : n - 1])
-    sent(9, summed_out)
 
 
 def split_shards(
@@ -1108,11 +1098,29 @@
     head_rows = 16
     bf16, f32 = jnp.bfloat16, jnp.float32
     dma = pltpu.SemaphoreType.DMA
+    operands = (
+        tokens,
+        mix_gain[None],
+        latent_gain[None],
+        head_gain[None],
+        conv_taps,
+        conv_b_weight,
+        conv_c_weight,
+        conv_v_weight,
+        query_weight,
+        query_rope_weight,
+        latent_weight,
+        key_rope_weight.T,
+        key_up_weight,
+        value_up_weight,
+        conv_out_weight,
+        attn_out_weight,
+    )
     result = pl.pallas_call(
         functools.partial(layer_kernel, n, orders(n)),
         out_shape=jax.ShapeDtypeStruct((share, columns), bf16),
         in_specs=[pl.BlockSpec(memory_space=pltpu.HBM)] * 16,
-        out_specs=pl.BlockSpec(memory_space=pltpu.HBM),
+        out_specs=pl.BlockSpec(memory_space=pltpu.VMEM),
         scratch_shapes=[
             pltpu.VMEM((2, length, wide), bf16),
             pltpu.VMEM((length, features), bf16),
@@ -1148,32 +1156,14 @@
             dma((8,)),
             dma((n, n)),
             dma((n + 1, n)),
-            dma((10,)),
+            dma((9,)),
             pltpu.VMEM((n, tr, out_rows), bf16),
-            pltpu.VMEM((share, columns), bf16),
         ],
         compiler_params=pltpu.CompilerParams(
-            collective_id=0, has_side_effects=True, vmem_limit_bytes=60 * 1024 * 1024
+            collective_id=0, has_side_effects=True, vmem_limit_bytes=40 * 1024 * 1024
         ),
         name="whole_layer",
-    )(
-        tokens,
-        mix_gain[None],
-        latent_gain[None],
-        head_gain[None],
-        conv_taps,
-        conv_b_weight,
-        conv_c_weight,
-        conv_v_weight,
-        query_weight,
-        query_rope_weight,
-        latent_weight,
-        key_rope_weight.T,
-        key_up_weight,
-        value_up_weight,
-        conv_out_weight,
-        attn_out_weight,
-    )
+    )(*(pltpu.with_memory_space_constraint(operand, pltpu.HBM) for operand in operands))
     return result[None]
 
 

time: 89.8 us -> 86.8 us (0.967)
  Pallas kernels: 87.9 us -> 85.9 us
  local copies, waits for them, and re-layouts: 1.72 us -> 0.73 us
    pallas_call x1, Pallas kernels: 87.9 us -> 85.9 us  [split_shards(): pl.pallas_call(functools.partial(layer_kernel, n, orders(n)), out_shape=j...]
    unnamed x1, local copies, waits for them, and re-layouts: 1.72 us -> 0.73 us
where the time goes in v3:
time: 86.8 us; the launch traced here: 86.6 us
  Pallas kernels  85.9 us (99%)
    pallas_call x1, Pallas kernels, split_shards(): pl.pallas_call(functools.partial(layer_kernel, n, orders(n)), out_shape=j...  85.9 us

profile of v3, /device:TPU:0, one launch (start us, length us, event | category | flops | bytes accessed | tf_op | source)
XLA Modules:
  0.0 86.6 jit_solution(6742105137504719221)
XLA Ops:
  0.0 85.9 %whole_layer.1 = bf16[80,2048]{1,0:T(8,128)(2,1)S(1)} custom-call(bf16[1,160,1024]{2,1,0:T(8,128)(2,1)} %tok_in.1, f32[1,2048]{1,0:T(1,128)} %bitcast.7, f32[1,512]{1,0:T(1,128)} %bitcast.9, f32[1,1024]{1,0:T(1,128)} %bitcast.8, f32[3,512]{1,0:T(4,128)} %taps_in.1, bf16[128,512]{1,0:T(8,128)(2,1)} %cb.1, bf16[128,512]{1,0:T(8,128)(2,1)} %cc.1, ...), custom_call_target="tpu_custom_call" | custom-call | tf_op jit(solution)/shard_map/whole_layer/pallas_call | solution.py:1119
  85.9 0.7 copy.18

commit v4 on v3

--- a/solution.py
+++ b/solution.py
@@ -275,7 +275,7 @@
     for z in (0, n - 1):
         by = [abs(z - d) for d in range(n)]
         g = columns
-        sent = [(by[d], g[k]) for d, k in ((1, 0), (1, 1), (2, 0), (2, 1), (1, 2), (3, 0), (3, 1), (3, 2), (3, 3), (2, 2), (2, 3), (1, 3))]
+        sent = [(by[d], g[k]) for d, k in ((1, 0), (1, 1), (2, 0), (2, 1), (3, 0), (3, 1), (3, 2), (3, 3), (1, 2), (2, 2), (2, 3), (1, 3))]
         slots[z] = sent
     for z in range(n):
         end = 0 if 2 * z < n else n - 1
@@ -979,11 +979,11 @@
         def pass_before():
             pass_first(step_block(before), step_column(before))
 
-        opens = (block_opens(i) == 1) | (column_opens(i) == 1)
+        early = (i == 1) | (i == 2)
         passes = is_end & (i >= 1) & (i <= n * (n - 1))
-        pl.when(passes & opens)(pass_before)
+        pl.when(passes & early)(pass_before)
         pl.when(block_opens(i) == 1)(lambda: features(dest))
-        pl.when(is_end & (i == 0))(lambda: process_half(arrive_at(2), half_last))
+        pl.when(passes & (i == third_block))(pass_before)
 
         @pl.when(column_opens(i) == 1)
         def _():
@@ -994,7 +994,8 @@
             mix[dest], wout[:, cut(g)], preferred_element_type=jnp.float32
         ).astype(jnp.bfloat16)
         pair_copy(dest, g).start()
-        pl.when(passes & jnp.logical_not(opens))(pass_before)
+        pl.when(passes & jnp.logical_not(early | (i == third_block)))(pass_before)
+        pl.when(is_end & (i == 0))(lambda: process_half(arrive_at(2), half_last))
         for k in range(2, n):
             pl.when(i == k - 2)(lambda k=k: relay_plane(1, order[1][k]))
 

time: 86.8 us -> 85.3 us (0.983)
  Pallas kernels: 85.9 us -> 84.4 us
    pallas_call x1, Pallas kernels: 85.9 us -> 84.4 us  [split_shards(): pl.pallas_call(functools.partial(layer_kernel, n, orders(n)), out_shape=j...]
where the time goes in v4:
time: 85.3 us; the launch traced here: 85.1 us
  Pallas kernels  84.4 us (99%)
    pallas_call x1, Pallas kernels, split_shards(): pl.pallas_call(functools.partial(layer_kernel, n, orders(n)), out_shape=j...  84.4 us

profile of v4, /device:TPU:0, one launch (start us, length us, event | category | flops | bytes accessed | tf_op | source)
XLA Modules:
  0.0 85.1 jit_solution(13510235647899232093)
XLA Ops:
  0.0 84.4 %whole_layer.1 = bf16[80,2048]{1,0:T(8,128)(2,1)S(1)} custom-call(bf16[1,160,1024]{2,1,0:T(8,128)(2,1)} %tok_in.1, f32[1,2048]{1,0:T(1,128)} %bitcast.7, f32[1,512]{1,0:T(1,128)} %bitcast.9, f32[1,1024]{1,0:T(1,128)} %bitcast.8, f32[3,512]{1,0:T(4,128)} %taps_in.1, bf16[128,512]{1,0:T(8,128)(2,1)} %cb.1, bf16[128,512]{1,0:T(8,128)(2,1)} %cc.1, ...), custom_call_target="tpu_custom_call" | custom-call | tf_op jit(solution)/shard_map/whole_layer/pallas_call | solution.py:1120
  84.4 0.7 copy.18

commit v5 on v4

--- a/solution.py
+++ b/solution.py
@@ -275,7 +275,7 @@
     for z in (0, n - 1):
         by = [abs(z - d) for d in range(n)]
         g = columns
-        sent = [(by[d], g[k]) for d, k in ((1, 0), (1, 1), (2, 0), (2, 1), (3, 0), (3, 1), (3, 2), (3, 3), (1, 2), (2, 2), (2, 3), (1, 3))]
+        sent = [(by[d], g[k]) for d, k in ((1, 0), (1, 1), (2, 0), (2, 1), (3, 0), (3, 1), (3, 2), (3, 3), (2, 2), (2, 3), (1, 2), (1, 3))]
         slots[z] = sent
     for z in range(n):
         end = 0 if 2 * z < n else n - 1

time: 85.3 us -> 85.3 us (level)
  no operation moved by 1% of the time
where the time goes in v5:
time: 85.3 us; the launch traced here: 85.1 us
  Pallas kernels  84.4 us (99%)
    pallas_call x1, Pallas kernels, split_shards(): pl.pallas_call(functools.partial(layer_kernel, n, orders(n)), out_shape=j...  84.4 us

profile of v5, /device:TPU:0, one launch (start us, length us, event | category | flops | bytes accessed | tf_op | source)
XLA Modules:
  0.0 85.1 jit_solution(14855786530869649402)
XLA Ops:
  0.0 84.4 %whole_layer.1 = bf16[80,2048]{1,0:T(8,128)(2,1)S(1)} custom-call(bf16[1,160,1024]{2,1,0:T(8,128)(2,1)} %tok_in.1, f32[1,2048]{1,0:T(1,128)} %bitcast.7, f32[1,512]{1,0:T(1,128)} %bitcast.9, f32[1,1024]{1,0:T(1,128)} %bitcast.8, f32[3,512]{1,0:T(4,128)} %taps_in.1, bf16[128,512]{1,0:T(8,128)(2,1)} %cb.1, bf16[128,512]{1,0:T(8,128)(2,1)} %cc.1, ...), custom_call_target="tpu_custom_call" | custom-call | tf_op jit(solution)/shard_map/whole_layer/pallas_call | solution.py:1120
  84.4 0.7 copy.18
